TPU v7x, 128 devices: a whole 4x4x4 slice. The times are simulated.
128 devices in a mesh: ep: 16 (over z, x), tp: 8 (over y, core).
Axes of the slice: x: 4, y: 4, z: 4, core: 2. Of those that a mesh axis runs over, the one named last changes fastest.
Arguments:
- mixer_input: bfloat16 [16384, 2048], P(('ep', 'tp')), may hold values from -6 to 6
- log_decay: float32 [16384, 8], P('ep', 'tp'), may hold values from -0.8 to 0
- mixer_gain: float32 [2048], replicated, may hold values from 0.1 to 1.9
- query_weight: bfloat16 [2048, 1024], P(None, 'tp'), may hold values from -0.125 to 0.125
- key_weight: bfloat16 [2048, 1024], P(None, 'tp'), may hold values from -0.125 to 0.125
- value_weight: bfloat16 [2048, 2048], P(None, 'tp'), may hold values from -0.125 to 0.125
- gate_weight: bfloat16 [2048, 2048], P(None, 'tp'), may hold values from -0.125 to 0.125
- head_gain: float32 [2048], P('tp'), may hold values from 0.1 to 1.9
- output_weight: bfloat16 [2048, 2048], P('tp'), may hold values from -0.125 to 0.125
- expert_input: bfloat16 [16384, 2048], P(('ep', 'tp')), may hold values from -6 to 6
- expert_gain: float32 [2048], replicated, may hold values from 0.1 to 1.9
- routes: int32 [16384, 2], P(('ep', 'tp')), may hold values from 0 to 127, as said below
- group_weight: float32 [16384], P(('ep', 'tp')), may hold values from 0.3 to 1
- pair_weight: float32 [16384, 2], P(('ep', 'tp')), may hold values from 0.2 to 1
- expert_gate: bfloat16 [128, 2048, 1024], P(('ep', 'tp')), may hold values from -0.125 to 0.125
- expert_up: bfloat16 [128, 2048, 1024], P(('ep', 'tp')), may hold values from -0.125 to 0.125
- expert_down: bfloat16 [128, 1024, 2048], P(('ep', 'tp')), may hold values from -0.1875 to 0.1875
Outputs:
- mixer_output: bfloat16 [16384, 2048], P(('ep', 'tp'))
- expert_output: bfloat16 [16384, 2048], P(('ep', 'tp'))
Inputs may be any that keep to these rules, and one draw needn't show every extreme that they name: `routes`: in the rows of one device each expert is named at most 3 times; one expert is named exactly 3 times in the rows of every device. A row names two different experts of the same group, a group being 32 consecutive expert numbers.
All inputs are finite; a program needn't handle non-finite values.
Results may differ from a plain program's by a relative error of at most 0.023.
Values may be sent and summed in bfloat16 or wider, within the bound.
A program may use at most 128 MiB of HBM per device.

v0:
```python
import jax
import jax.numpy as jnp
from jax import lax
from jax.sharding import PartitionSpec as P

KEY_DIM = 128
VALUE_DIM = 256
SPAN = 512
TOPK = 2


EPSILON = 1e-05
THETA = 10000.0


def from_everyone(shard, axis):
    copies = jnp.broadcast_to(shard, (lax.axis_size(axis), *shard.shape))
    return lax.all_to_all(copies, axis, split_axis=0, concat_axis=0, tiled=True)


def combined_pairwise(pieces, combine):
    while len(jax.tree.leaves(pieces)[0]) > 1:
        pieces = jax.vmap(combine)(
            *(jax.tree.map(lambda part: part[side::2], pieces) for side in (0, 1))
        )
    return jax.tree.map(lambda part: part[0], pieces)


def entering(shard, axis, combine, identity):
    size, position = (lax.axis_size(axis), lax.axis_index(axis))
    passed = jnp.arange(size) < position

    def kept(part, zero, own):
        part = jnp.where(
            passed.reshape(-1, *(1 for _ in own.shape)),
            part.astype(own.dtype),
            jnp.asarray(zero, own.dtype),
        )
        return part

    pieces = jax.tree.map(
        lambda part: from_everyone(part, axis),
        jax.tree.map(lambda part, kind: part.astype(kind), shard, (jnp.bfloat16, jnp.bfloat16)),
    )
    return combined_pairwise(jax.tree.map(kept, pieces, identity, shard), combine)


def split_up(shard, dim, size):
    before, after = (shard.shape[:dim], shard.shape[dim + 1 :])
    return jnp.moveaxis(shard.reshape(*before, size, -1, *after), dim, 0)


def sum_at_owner(shard, axis, dim):
    blocks = split_up(shard, dim, lax.axis_size(axis))
    arrived = lax.all_to_all(blocks, axis, split_axis=0, concat_axis=0, tiled=True)
    return arrived.astype(jnp.float32).sum(axis=0)


def joined_along(blocks, dim):
    blocks = jnp.moveaxis(blocks, 0, dim)
    dims = blocks.shape
    return blocks.reshape(*dims[:dim], dims[dim] * dims[dim + 1], *dims[dim + 2 :])


def joined_exchange(shard, axis, axes, splits, concats):
    sizes = [lax.axis_size(a) for a in axes]
    blocks = split_up(shard, splits[0], sizes[0])
    blocks = jnp.moveaxis(split_up(blocks, splits[1] + 1, sizes[1]), 0, 1)
    inside = blocks.shape[2:]
    blocks = blocks.reshape(-1, *inside)
    blocks = lax.all_to_all(blocks, axis, split_axis=0, concat_axis=0, tiled=True)
    blocks = joined_along(blocks.reshape(*sizes, *inside), concats[0] + 1)
    return joined_along(blocks, concats[1])


def layer_norm(matrix, norm_gain):
    matrix = matrix.astype(jnp.float32)
    average = jnp.mean(matrix, axis=-1, keepdims=True)
    centred = matrix - average
    spread = jnp.mean(centred * centred, axis=-1, keepdims=True)
    return centred * lax.rsqrt(spread + EPSILON) * norm_gain


def rotate(values, position):
    halfway = values.shape[-1] // 2
    frequency = THETA ** (-jnp.arange(halfway, dtype=jnp.float32) / halfway)
    angles = position[:, None] * frequency[None, :]
    cosine = jnp.cos(angles)[:, None, :]
    sine_part = jnp.sin(angles)[:, None, :]
    leading = values[..., :halfway]
    trailing = values[..., halfway:]
    return jnp.concatenate(
        [leading * cosine - trailing * sine_part, trailing * cosine + leading * sine_part], axis=-1
    )


def block_step(state, inputs):
    query_rows, key_rows, value_rows, decay_factor = inputs
    span_len = query_rows.shape[0]
    cumulative = jnp.cumsum(decay_factor, axis=0)
    causal = jnp.arange(span_len)[:, None] >= jnp.arange(span_len)[None, :]
    log_gaps = cumulative.T[:, :, None] - cumulative.T[:, None, :]
    weight = jnp.where(causal[None], jnp.exp(jnp.minimum(log_gaps, 0.0)), 0.0)
    scores = jnp.einsum("thd,shd->hts", query_rows, key_rows, preferred_element_type=jnp.float32)
    decayed = (scores * weight).astype(jnp.bfloat16)
    within = jnp.einsum("hts,she->the", decayed, value_rows, preferred_element_type=jnp.float32)
    scaled = query_rows.astype(jnp.float32) * jnp.exp(cumulative)[:, :, None]
    carried = jnp.einsum("thd,hde->the", scaled, state)
    span_total = cumulative[-1]
    remain = jnp.exp(span_total[None, :] - cumulative)
    weighted_keys = key_rows.astype(jnp.float32) * remain[:, :, None]
    update = jnp.einsum("shd,she->hde", weighted_keys, value_rows.astype(jnp.float32))
    return (state * jnp.exp(span_total)[:, None, None] + update, within + carried)


def token_mixer(
    mixer_input,
    log_decay,
    mixer_gain,
    query_weight,
    key_weight,
    value_weight,
    gate_weight,
    head_gain,
    output_weight,
):
    normed = layer_norm(mixer_input, mixer_gain).astype(jnp.bfloat16)
    key_cols = query_weight.shape[1]
    value_cols = value_weight.shape[1]
    row_piece = lax.all_gather(normed, "tp", axis=0, tiled=True)
    pieces = [
        jnp.dot(row_piece, weight, preferred_element_type=jnp.float32).astype(jnp.bfloat16)
        for weight in (query_weight, key_weight, value_weight, gate_weight)
    ]
    projected = jnp.concatenate(pieces, axis=1)
    seg_rows = projected.shape[0]
    heads_dev = key_cols // KEY_DIM
    query_rows = projected[:, :key_cols].reshape(seg_rows, heads_dev, KEY_DIM)
    key_rows = projected[:, key_cols : 2 * key_cols].reshape(seg_rows, heads_dev, KEY_DIM)
    value_rows = projected[:, 2 * key_cols : 2 * key_cols + value_cols].reshape(
        seg_rows, heads_dev, VALUE_DIM
    )
    gate_rows = projected[:, 2 * key_cols + value_cols :].astype(jnp.float32)
    position = (lax.axis_index("ep") * seg_rows + jnp.arange(seg_rows, dtype=jnp.int32)).astype(
        jnp.float32
    )
    rot_query = rotate(query_rows.astype(jnp.float32), position).astype(jnp.bfloat16)
    rot_key = rotate(key_rows.astype(jnp.float32), position).astype(jnp.bfloat16)
    blocks = seg_rows // SPAN

    def split_blocks(tensor):
        return tensor.reshape((blocks, SPAN) + tensor.shape[1:])

    state_zero = jnp.zeros((heads_dev, KEY_DIM, VALUE_DIM), jnp.float32)
    local_state, local_out = lax.scan(
        block_step,
        state_zero,
        (
            split_blocks(rot_query),
            split_blocks(rot_key),
            split_blocks(value_rows),
            split_blocks(log_decay),
        ),
    )
    local_out = local_out.reshape(seg_rows, heads_dev, VALUE_DIM)
    running = jnp.cumsum(log_decay, axis=0)

    def combine(earlier, later):
        return (earlier[0] + later[0], earlier[1] * jnp.exp(later[0])[:, None, None] + later[1])

    identity = (jnp.zeros((heads_dev,), jnp.float32), state_zero)
    incoming = entering((running[-1], local_state), "ep", combine, identity)
    scaled_query = rot_query.astype(jnp.float32) * jnp.exp(running)[:, :, None]
    retained = local_out + jnp.einsum("thd,hde->the", scaled_query, incoming[1])
    average = jnp.mean(retained, axis=-1, keepdims=True)
    centred = retained - average
    spread = jnp.mean(centred * centred, axis=-1, keepdims=True)
    normed_heads = centred * lax.rsqrt(spread + EPSILON) * head_gain.reshape(heads_dev, VALUE_DIM)
    gated = (jax.nn.silu(gate_rows) * normed_heads.reshape(seg_rows, value_cols)).astype(
        jnp.bfloat16
    )
    summed = sum_at_owner(
        jnp.dot(gated, output_weight, preferred_element_type=jnp.float32).astype(jnp.bfloat16),
        "tp",
        0,
    )
    return summed.astype(jnp.bfloat16)


def expert_mixture(
    expert_input,
    expert_gain,
    routes,
    group_weight,
    pair_weight,
    expert_gate,
    expert_up,
    expert_down,
):
    normed = layer_norm(expert_input, expert_gain).astype(jnp.bfloat16)
    tok_rows = expert_input.shape[0]
    width = expert_input.shape[1]
    ep_count = lax.axis_size("ep")
    tp_count = lax.axis_size("tp")
    expert_count = ep_count * tp_count
    capacity = 3 * tok_rows * TOPK // (2 * expert_count)
    assigned = routes.reshape(-1)
    onehot = (assigned[:, None] == jnp.arange(expert_count, dtype=jnp.int32)[None, :]).astype(
        jnp.int32
    )
    earlier_hits = jnp.cumsum(onehot, axis=0) - onehot
    slot_rank = jnp.sum(earlier_hits * onehot, axis=1)
    destination = assigned * capacity + slot_rank
    slot_source = (
        jnp.zeros((expert_count * capacity,), jnp.int32)
        .at[destination]
        .set(jnp.arange(tok_rows * TOPK, dtype=jnp.int32) // TOPK)
    )
    slot_filled = jnp.zeros((expert_count * capacity,), jnp.bool_).at[destination].set(True)
    outgoing = jnp.where(slot_filled[:, None], normed[slot_source], jnp.zeros((), jnp.bfloat16))
    gate_matrix = expert_gate[0]
    up_matrix = expert_up[0]
    down_matrix = expert_down[0]
    sectioned = outgoing.reshape(ep_count, tp_count, capacity, width)
    arrived = joined_exchange(sectioned, ("ep", "tp"), ("ep", "tp"), (0, 1), (0, 1))
    flat_rows = arrived.reshape(-1, width)
    gate_part = jnp.dot(flat_rows, gate_matrix, preferred_element_type=jnp.float32)
    up_part = jnp.dot(flat_rows, up_matrix, preferred_element_type=jnp.float32)
    hidden = (jax.nn.silu(gate_part) * up_part).astype(jnp.bfloat16)
    results = joined_exchange(
        jnp.dot(hidden, down_matrix, preferred_element_type=jnp.float32)
        .astype(jnp.bfloat16)
        .reshape(arrived.shape),
        ("ep", "tp"),
        ("ep", "tp"),
        (0, 1),
        (0, 1),
    )
    returned_rows = (
        results.reshape(expert_count * capacity, width)[destination]
        .astype(jnp.float32)
        .reshape(tok_rows, TOPK, width)
    )
    mixing = group_weight[:, None] * pair_weight
    return jnp.sum(returned_rows * mixing[:, :, None], axis=1).astype(jnp.bfloat16)


def local(
    mixer_input,
    log_decay,
    mixer_gain,
    query_weight,
    key_weight,
    value_weight,
    gate_weight,
    head_gain,
    output_weight,
    expert_input,
    expert_gain,
    routes,
    group_weight,
    pair_weight,
    expert_gate,
    expert_up,
    expert_down,
):
    mixer_output = token_mixer(
        mixer_input,
        log_decay,
        mixer_gain,
        query_weight,
        key_weight,
        value_weight,
        gate_weight,
        head_gain,
        output_weight,
    )
    expert_output = expert_mixture(
        expert_input,
        expert_gain,
        routes,
        group_weight,
        pair_weight,
        expert_gate,
        expert_up,
        expert_down,
    )
    return (mixer_output, expert_output)


def solution(mesh):
    return jax.shard_map(
        local,
        mesh=mesh,
        in_specs=(
            P(("ep", "tp"), None),
            P("ep", "tp"),
            P(),
            P(None, "tp"),
            P(None, "tp"),
            P(None, "tp"),
            P(None, "tp"),
            P("tp"),
            P("tp", None),
            P(("ep", "tp"), None),
            P(),
            P(("ep", "tp"), None),
            P(("ep", "tp")),
            P(("ep", "tp"), None),
            P(("ep", "tp"), None, None),
            P(("ep", "tp"), None, None),
            P(("ep", "tp"), None, None),
        ),
        out_specs=(P(("ep", "tp"), None), P(("ep", "tp"), None)),
        check_vma=False,
    )
```

profile of v0, /device:TPU:1, one launch (start us, length us, event | category | flops | bytes accessed | tf_op | source)
XLA Modules:
  0.0 235.4 jit_solution(17247582961159877925)
XLA Ops:
  7.3 1.3 convert_reduce_fusion.1
  8.6 1.3 fusion.67
  9.9 2.2 fusion.69
  12.9 0.6 slice.125
  13.5 0.6 slice.124
  15.3 0.6 broadcast_in_dim.57
  15.9 8.4 %all-to-all-start.1 = ((bf16[16,1,1]{2,1,0:T(2,128)(2,1)}), bf16[16,1,1]{2,1,0:T(2,128)(2,1)S(1)}, u32[]{:S(2)}, u32[]{:S(2)}) async-start(bf16[16,1,1]{2,1,0:T(2,128)(2,1)} %broadcast_in_dim.57), calls=%async_computation.1 | async-start | bytes 16384 | tf_op jit(solution)/shard_map/all_to_all | solution.py:18
  25.7 1.4 scatter_custom_fusion.1
  27.6 0.4 fusion.66
  28.0 3.1 %gather_fusion = bf16[384,2048]{1,0:T(8,128)(2,1)} fusion(bf16[128,2048]{1,0:T(8,128)(2,1)S(1)} %fusion.66, s32[1024]{0:T(1024)S(1)} %pad_clamp_fusion.1), kind=kCustom, calls=%fused_computation | custom fusion | bytes 3147264 | tf_op jit(solution)/shard_map/gather | solution.py:220
  31.1 4.0 %gather.9 = bf16[128,1,1,3,2048]{4,3,0,2,1:T(4,128)(2,1)S(1)} reshape(bf16[384,2048]{1,0:T(8,128)(2,1)} %gather_fusion) | data formatting | bytes 3145728 | tf_op jit(solution)/shard_map/gather | solution.py:220
  35.2 1.5 scatter_custom_fusion
  36.9 2.4 %select_bitcast_fusion = bf16[128,1,1,3,2048]{4,3,2,1,0:T(4,128)(2,1)} fusion(bf16[128,1,1,3,2048]{4,3,0,2,1:T(4,128)(2,1)S(1)} %gather.9, pred[128,3]{1,0:T(8,128)(4,1)S(1)} %broadcast_in_dim.61), kind=kLoop, calls=%fused_computation.62 | loop fusion | flops 786432 | bytes 3146112 | tf_op jit(solution)/shard_map/jit(_where)/select_n | solution.py:220
  39.3 10.3 %all-to-all-start.3 = ((bf16[128,1,1,3,2048]{4,3,2,1,0:T(4,128)(2,1)}), bf16[128,1,1,3,2048]{4,3,2,1,0:T(4,128)(2,1)S(1)}, u32[]{:S(2)}, u32[]{:S(2)}) async-start(bf16[128,1,1,3,2048]{4,3,2,1,0:T(4,128)(2,1)} %select_bitcast_fusion), calls=%async_computation.3 | async-start | bytes 4194304 | tf_op jit(solution)/shard_map/all_to_all | solution.py:71
  49.6 0.5 iota_compare_fusion.3
  50.1 0.7 fusion.117
  51.2 0.6 fusion.128
  52.0 0.5 fusion.127
  52.7 0.6 fusion.126
  53.2 0.6 slice.107
  54.6 25.1 %all-to-all-done.3 = bf16[128,1,1,3,2048]{4,3,2,1,0:T(4,128)(2,1)S(1)} async-done(((bf16[128,1,1,3,2048]{4,3,2,1,0:T(4,128)(2,1)}), bf16[128,1,1,3,2048]{4,3,2,1,0:T(4,128)(2,1)S(1)}, u32[]{:S(2)}, u32[]{:S(2)}) %all-to-all-start.3) | async-done | bytes 1572896 | tf_op jit(solution)/shard_map/all_to_all | solution.py:71
  79.7 2.5 %reshape_reshape.10 = bf16[384,2048]{1,0:T(8,128)(2,1)} reshape(bf16[16,8,1,3,2048]{4,3,1,0,2:T(4,128)(2,1)S(1)} %bitcast.228) | data formatting | bytes 3145728 | tf_op jit(solution)/shard_map/reshape;reshape | solution.py:226
  82.2 5.7 %fusion.48 = f32[384,1024]{1,0:T(8,128)} fusion(bf16[384,2048]{1,0:T(8,128)(2,1)} %reshape_reshape.10, bf16[1,2048,1024]{2,1,0:T(8,128)(2,1)} %param.33), kind=kOutput, calls=%fused_computation.57 | convolution fusion | flops 1610612736 | bytes 7340032 | tf_op jit(solution)/shard_map/dot_general | solution.py:227
  87.9 3.9 %fusion.61 = f32[1024,1,128]{0,2,1:T(8,128)S(1)} fusion(bf16[1024,2048]{1,0:T(8,128)(2,1)} %all-gather.2.cloned.1.call-done, bf16[2048,128]{1,0:T(8,128)(2,1)S(1)} %copy-done.7), kind=kOutput, calls=%fused_computation.82 | convolution fusion | flops 537133056 | bytes 5242880 | tf_op jit(solution)/shard_map/dot_general | solution.py:132
  91.8 1.5 fusion.63
  93.3 1.2 fusion.102
  95.5 3.7 %convolution_convert_fusion.1 = bf16[1024,256]{1,0:T(8,128)(2,1)S(1)} fusion(bf16[1024,2048]{1,0:T(8,128)(2,1)} %all-gather.2.cloned.1.call-done, bf16[2048,256]{1,0:T(8,128)(2,1)} %param.24), kind=kOutput, calls=%fused_computation.73 | convolution fusion | flops 1074003968 | bytes 5767168 | tf_op jit(solution)/shard_map/dot_general | solution.py:132
  99.3 11.5 %while.13 = (s32[]{:T(128)}, f32[1,128,256]{2,1,0:T(8,128)S(1)}, f32[2,512,1,256]{3,1,0,2:T(8,128)}, f32[2,512,1]{1,2,0:T(1,128)S(1)}, bf16[2,512,1,128]{3,1,2,0...) while((s32[]{:T(128)}, f32[1,128,256]{2,1,0:T(8,128)S(1)}, ...), condition=%wide.region_5.6_spmd.clone, body=%wide.region_2.5_spmd.clone.sunk | while | flops 270598656 | bytes 5144364 | solution.py:155
  99.3 0.3 reduce-window.39
  100.1 0.4 convolution_bitcast_fusion.4
  100.4 0.6 fusion.160
  101.2 0.8 constant_dynamic-update-slice_fusion.2
  102.1 0.6 slice.167
  102.7 0.6 slice.166
  104.6 0.3 fusion.159
  105.8 0.4 convolution_bitcast_fusion.4
  106.1 0.6 fusion.160
  106.9 0.9 constant_dynamic-update-slice_fusion.2
  107.8 0.6 slice.167
  108.5 0.6 slice.166
  110.4 0.3 fusion.159
  110.8 1.2 broadcast_in_dim.55
  111.9 3.7 %all-to-all-start = ((bf16[16,1,128,256]{3,2,1,0:T(8,128)(2,1)}), bf16[16,1,128,256]{3,2,1,0:T(8,128)(2,1)S(1)}, u32[]{:S(2)}, u32[]{:S(2)}) async-start(bf16[16,1,128,256]{3,2,1,0:T(8,128)(2,1)} %broadcast_in_dim.55), calls=%async_computation | async-start | bytes 2097152 | tf_op jit(solution)/shard_map/all_to_all | solution.py:18
  115.6 9.1 %fusion.50 = bf16[384,2048]{1,0:T(8,128)(2,1)} fusion(bf16[1,1024,2048]{2,1,0:T(8,128)(2,1)} %param.35, f32[384,1024]{1,0:T(8,128)} %fusion.48, bf16[384,2048]{1,0:T(8,128)(2,1)} %reshape_reshape.10, bf16[1,2048,1024]{2,1,0:T(8,128)(2,1)} %param.34), kind=kOutput, calls=%fused_computation.60 | convolution fusion | flops 3224371200 | bytes 13107200 | tf_op jit(solution)/shard_map/dot_general | solution.py:231
  124.6 5.2 %reshape_transpose_transpose_reshape_reshape_reshape.4 = bf16[128,1,1,3,2048]{4,3,0,2,1:T(4,128)(2,1)} reshape(bf16[384,2048]{1,0:T(8,128)(2,1)} %fusion.50) | data formatting | bytes 3145728 | tf_op jit(solution)/shard_map/reshape;transpose;transpose;reshape;reshape;reshape | solution.py:70
  129.8 1.4 all-to-all-done
  131.2 1.0 copy-done.4
  132.2 6.5 %all-to-all-start.4 = ((bf16[128,1,1,3,2048]{4,3,2,1,0:T(4,128)(2,1)}), bf16[128,1,1,3,2048]{4,3,2,1,0:T(4,128)(2,1)S(1)}, u32[]{:S(2)}, u32[]{:S(2)}) async-start(bf16[128,1,1,3,2048]{4,3,2,1,0:T(4,128)(2,1)} %bitcast.229), calls=%async_computation.4 | async-start | bytes 4194304 | tf_op jit(solution)/shard_map/all_to_all | solution.py:71
  138.8 1.5 convert_select_fusion
  140.5 0.3 copy-done.15
  141.1 0.4 copy-done.6
  141.5 0.5 fusion.129
  142.0 1.0 copy-done.5
  143.0 0.4 multiply_reduce_fusion.1
  143.4 9.3 %convolution_convert_fusion = bf16[1024,2048]{1,0:T(8,128)(2,1)} fusion(bf16[256,2048]{1,0:T(8,128)(2,1)S(1)} %copy-done, bf16[1024,2048]{1,0:T(8,128)(2,1)} %all-gather.2.cloned.1.call-done, bf16[2048,256]{1,0:T(8,128)(2,1)} %param.25, f32[1024,1,256]{2,0,1:T(8,128)} %copy-done.5, f32[256]{0:T(256)S(1)} %copy-done.21, f32[1024]{0:T(1024)S(1)} %add_rsqrt_fusion, ...), kind=kOutput, calls=%fused_computation.59 | convolution fusion | flops 2152464384 | bytes 11543552 | tf_op jit(solution)/shard_map/dot_general | solution.py:183
  152.7 16.2 %all-to-all-done.4 = bf16[128,1,1,3,2048]{4,3,2,1,0:T(4,128)(2,1)S(1)} async-done(((bf16[128,1,1,3,2048]{4,3,2,1,0:T(4,128)(2,1)}), bf16[128,1,1,3,2048]{4,3,2,1,0:T(4,128)(2,1)S(1)}, u32[]{:S(2)}, u32[]{:S(2)}) %all-to-all-start.4) | async-done | bytes 1572896 | tf_op jit(solution)/shard_map/all_to_all | solution.py:71
  168.9 1.3 copy-done.2
  170.2 5.7 %all-to-all-start.2 = ((bf16[8,128,2048]{2,1,0:T(8,128)(2,1)}), bf16[8,128,2048]{2,1,0:T(8,128)(2,1)}, u32[]{:S(2)}, u32[]{:S(2)}) async-start(bf16[8,128,2048]{2,1,0:T(8,128)(2,1)} %bitcast.230), calls=%async_computation.2 | async-start | bytes 8388608 | tf_op jit(solution)/shard_map/all_to_all | solution.py:55
  176.1 3.9 %reshape_reshape.11 = bf16[384,2048]{1,0:T(8,128)(2,1)S(1)} reshape(bf16[16,8,1,3,2048]{4,3,1,0,2:T(4,128)(2,1)} %bitcast.227) | data formatting | bytes 3145728 | tf_op jit(solution)/shard_map/reshape;reshape | solution.py:240
  180.0 2.3 gather_fusion.1
  182.3 2.4 %reshape.824 = f32[128,2,2048]{2,1,0:T(2,128)S(1)} reshape(bf16[256,2048]{1,0:T(8,128)(2,1)} %gather_fusion.1) | data formatting | bytes 3145728 | tf_op jit(solution)/shard_map/convert_element_type | solution.py:241
  184.7 3.9 %multiply_reduce_fusion = bf16[128,2048]{1,0:T(8,128)(2,1)} fusion(f32[128,2,2048]{2,1,0:T(2,128)S(1)} %reshape.824, f32[128,2]{1,0:T(8,128)S(1)} %copy.73), kind=kLoop, calls=%fused_computation.61 | loop fusion | flops 786432 | bytes 2622464 | tf_op jit(solution)/shard_map/reduce_sum | solution.py:245
  188.6 36.1 %all-to-all-done.2 = bf16[8,128,2048]{2,1,0:T(8,128)(2,1)} async-done(((bf16[8,128,2048]{2,1,0:T(8,128)(2,1)}), bf16[8,128,2048]{2,1,0:T(8,128)(2,1)}, u32[]{:S(2)}, u32[]{:S(2)}) %all-to-all-start.2) | async-done | bytes 4194336 | tf_op jit(solution)/shard_map/all_to_all | solution.py:55
  224.7 3.8 %reduce_sum.90 = bf16[128,2048]{1,0:T(8,128)(2,1)} reduce(bf16[8,128,2048]{2,1,0:T(8,128)(2,1)} %all-to-all-done.2, bf16[]{:T(256)} %constant.88.clone.1), dimensions={0}, to_apply=%region_10.11 | reduce | flops 1835008 | bytes 4718594 | tf_op jit(solution)/shard_map/reduce_sum | solution.py:56
  (118 shorter events, 6.9 us)
Async XLA Ops:
  7.2 136.2 %copy-start = (bf16[256,2048]{1,0:T(8,128)(2,1)S(1)}, bf16[256,2048]{1,0:T(8,128)(2,1)}, u32[]{:S(2)}) copy-start(bf16[256,2048]{1,0:T(8,128)(2,1)} %param.27) | copy-start | bytes 3145732
  7.2 5.0 %copy-start.9 = (f32[1024,1]{0,1:T(1,128)S(1)}, f32[1024,1]{0,1:T(1,128)}, u32[]{:S(2)}) copy-start(f32[1024,1]{0,1:T(1,128)} %param.20) | copy-start | bytes 12292
  7.2 17.2 %copy-start.12 = (s32[128,2]{0,1:T(2,128)S(1)}, s32[128,2]{0,1:T(2,128)}, u32[]{:S(2)}) copy-start(s32[128,2]{0,1:T(2,128)} %param.30) | copy-start | bytes 3076
  7.2 19.9 %copy-start.3 = (bf16[128,2048]{1,0:T(8,128)(2,1)S(1)}, bf16[128,2048]{1,0:T(8,128)(2,1)}, u32[]{:S(2)}) copy-start(bf16[128,2048]{1,0:T(8,128)(2,1)} %param.28) | copy-start | bytes 1572868
  7.2 80.7 %all-gather.2.cloned.1.call-start = ((), (), s32[]{:S(2)}) async-start(), calls=%async_computation.5 | async-start | bytes 4718592 | tf_op jit(solution)/shard_map/all_gather | solution.py:130
  9.9 17.7 %copy-start.11 = (f32[2048]{0:T(1024)S(1)}, f32[2048]{0:T(1024)}, u32[]{:S(2)}) copy-start(f32[2048]{0:T(1024)} %param.29) | copy-start | bytes 24580
  15.9 23.3 %all-to-all-start.1 = ((bf16[16,1,1]{2,1,0:T(2,128)(2,1)}), bf16[16,1,1]{2,1,0:T(2,128)(2,1)S(1)}, u32[]{:S(2)}, u32[]{:S(2)}) async-start(bf16[16,1,1]{2,1,0:T(2,128)(2,1)} %broadcast_in_dim.57), calls=%async_computation.1 | async-start | bytes 16384 | tf_op jit(solution)/shard_map/all_to_all | solution.py:18
  25.7 9.5 %copy-start.13 = (s32[256,1]{0,1:T(1,128)}, s32[256,1]{0,1:T(1,128)S(1)}, u32[]{:S(2)}) copy-start(s32[256,1]{0,1:T(1,128)S(1)} %compare_select_fusion) | copy-start | bytes 3076
  39.3 40.4 %all-to-all-start.3 = ((bf16[128,1,1,3,2048]{4,3,2,1,0:T(4,128)(2,1)}), bf16[128,1,1,3,2048]{4,3,2,1,0:T(4,128)(2,1)S(1)}, u32[]{:S(2)}, u32[]{:S(2)}) async-start(bf16[128,1,1,3,2048]{4,3,2,1,0:T(4,128)(2,1)} %select_bitcast_fusion), calls=%async_computation.3 | async-start | bytes 4194304 | tf_op jit(solution)/shard_map/all_to_all | solution.py:71
  82.2 5.7 %copy-start.7 = (bf16[2048,128]{1,0:T(8,128)(2,1)S(1)}, bf16[2048,128]{1,0:T(8,128)(2,1)}, u32[]{:S(2)}) copy-start(bf16[2048,128]{1,0:T(8,128)(2,1)} %param.23) | copy-start | bytes 1572868
  87.9 3.9 %copy-start.8 = (bf16[2048,128]{1,0:T(8,128)(2,1)S(1)}, bf16[2048,128]{1,0:T(8,128)(2,1)}, u32[]{:S(2)}) copy-start(bf16[2048,128]{1,0:T(8,128)(2,1)} %param.22) | copy-start | bytes 1572868
  87.9 3.9 %copy-start.1 = (bf16[1024,2048]{1,0:T(8,128)(2,1)S(1)}, bf16[1024,2048]{1,0:T(8,128)(2,1)}, u32[]{:S(2)}) copy-start(bf16[1024,2048]{1,0:T(8,128)(2,1)} %all-gather.2.cloned.1.call-done) | copy-start | bytes 12582916
  111.9 19.3 %all-to-all-start = ((bf16[16,1,128,256]{3,2,1,0:T(8,128)(2,1)}), bf16[16,1,128,256]{3,2,1,0:T(8,128)(2,1)S(1)}, u32[]{:S(2)}, u32[]{:S(2)}) async-start(bf16[16,1,128,256]{3,2,1,0:T(8,128)(2,1)} %broadcast_in_dim.55), calls=%async_computation | async-start | bytes 2097152 | tf_op jit(solution)/shard_map/all_to_all | solution.py:18
  131.2 1.0 copy-start.4
  131.2 7.5 %copy-start.20 = (pred[16]{0:T(512)(128)(4,1)S(1)}, pred[16]{0:T(512)(128)(4,1)}, u32[]{:S(2)}) copy-start(pred[16]{0:T(512)(128)(4,1)} %iota_compare_fusion.3) | copy-start | bytes 52
  132.2 36.6 %all-to-all-start.4 = ((bf16[128,1,1,3,2048]{4,3,2,1,0:T(4,128)(2,1)}), bf16[128,1,1,3,2048]{4,3,2,1,0:T(4,128)(2,1)S(1)}, u32[]{:S(2)}, u32[]{:S(2)}) async-start(bf16[128,1,1,3,2048]{4,3,2,1,0:T(4,128)(2,1)} %bitcast.229), calls=%async_computation.4 | async-start | bytes 4194304 | tf_op jit(solution)/shard_map/all_to_all | solution.py:71
  138.8 1.5 copy-start.17
  140.3 0.6 copy-start.15
  140.3 0.7 copy-start.16
  140.3 1.2 copy-start.6
  140.3 1.2 copy-start.10
  141.0 2.3 copy-start.21
  142.0 1.0 copy-start.5
  168.9 1.3 copy-start.2
  168.9 7.0 %copy-start.18 = (f32[128,2]{0,1:T(2,128)S(1)}, f32[128,2]{0,1:T(2,128)}, u32[]{:S(2)}) copy-start(f32[128,2]{0,1:T(2,128)} %param.32) | copy-start | bytes 3076
  168.9 7.0 %copy-start.19 = (f32[128]{0:T(128)S(1)}, f32[128]{0:T(128)}, u32[]{:S(2)}) copy-start(f32[128]{0:T(128)} %param.31) | copy-start | bytes 1540
  168.9 7.2 %copy-start.14 = (s32[256,1]{0,1:T(1,128)S(1)}, s32[256,1]{0,1:T(1,128)}, u32[]{:S(2)}) copy-start(s32[256,1]{0,1:T(1,128)} %copy-done.13) | copy-start | bytes 3076
  170.2 54.5 %all-to-all-start.2 = ((bf16[8,128,2048]{2,1,0:T(8,128)(2,1)}), bf16[8,128,2048]{2,1,0:T(8,128)(2,1)}, u32[]{:S(2)}, u32[]{:S(2)}) async-start(bf16[8,128,2048]{2,1,0:T(8,128)(2,1)} %bitcast.230), calls=%async_computation.2 | async-start | bytes 8388608 | tf_op jit(solution)/shard_map/all_to_all | solution.py:55
Sparse Core Ops, SparseCore 0:
  12.3 35.6 all-gather.1
where the time goes:
time: 236 us; the launch traced here: 235 us
  waiting for transfers between devices  78.8 us (33%)
  local copies, waits for them, and re-layouts  41.7 us (18%)
  matrix products  36.1 us (15%)
  starting transfers between devices  34.6 us (15%)
  other arithmetic  24.8 us (11%)
  between operations  16.5 us (7%)
  loops' own time  2.79 us (1%)
    all_to_all x2, waiting for transfers between devices, joined_exchange(): lax.all_to_all(blocks, axis, split_axis=0, concat_axis=0, tiled=True)  41.3 us
    all_to_all x1, waiting for transfers between devices, sum_at_owner(): lax.all_to_all(blocks, axis, split_axis=0, concat_axis=0, tiled=True)  36.1 us
    all_to_all x2, starting transfers between devices, joined_exchange(): lax.all_to_all(blocks, axis, split_axis=0, concat_axis=0, tiled=True)  16.8 us
    all_to_all x2, starting transfers between devices, from_everyone(): return lax.all_to_all(copies, axis, split_axis=0, concat_axis=0, tiled=True)  12.1 us
    dot_general x1, matrix products, token_mixer(): jnp.dot(gated, output_weight, preferred_element_type=jnp.float32)  9.28 us
    dot_general x3, matrix products, token_mixer(): jnp.dot(row_piece, weight, preferred_element_type=jnp.float32)  9.11 us
    dot_general x1, matrix products, expert_mixture(): jnp.dot(hidden, down_matrix, preferred_element_type=jnp.float32)  9.05 us
    gather x2, local copies, waits for them, and re-layouts, expert_mixture(): normed[slot_source]  7.15 us
  transfers between devices with their start and end apart: 6, of which 4 were waited for; matrix products, arithmetic and copies ran while one was open for 29% of the time, Pallas kernels for 0%

commit v1 on v0

v1 whole, which is shorter than its diff:
```python
import functools

import jax
import jax.numpy as jnp
import numpy as np
from jax import lax
from jax.experimental import pallas as pl
from jax.experimental.pallas import tpu as pltpu
from jax.sharding import PartitionSpec as P

KD = 128
VD = 256
CAP = 3
EPSILON = 1e-05
THETA = 10000.0
CHUNKS = 4
MESH = pl.DeviceIdType.MESH
F32 = jnp.float32
BF16 = jnp.bfloat16
HI = lax.Precision.HIGHEST


def dot(a, b, **kw):
    return jnp.dot(a, b, preferred_element_type=F32, **kw)


def dot_t0(a, b):
    return lax.dot_general(a, b, (((0,), (0,)), ((), ())), preferred_element_type=F32)


def dot_t1(a, b):
    return lax.dot_general(a, b, (((1,), (1,)), ((), ())), preferred_element_type=F32)


def norm_rows(src, gain, dst, rows, step):
    @pl.loop(0, rows // step)
    def _(i):
        at = pl.ds(pl.multiple_of(i * step, step), step)
        m = src[at, :].astype(F32)
        mean = jnp.mean(m, axis=-1, keepdims=True)
        c = m - mean
        var = jnp.mean(c * c, axis=-1, keepdims=True)
        dst[at, :] = (c * lax.rsqrt(var + EPSILON) * gain[...]).astype(BF16)


def rows_of(x3):
    a, b, c = x3.shape
    return x3.astype(F32).reshape(a * b, c).astype(BF16)


def kernel(
    dims,
    x_ref, ld_ref, mgain_ref, wq_ref, wk_ref, wv_ref, wg_ref, hgain_ref, wo_ref,
    e_ref, egain_ref, routes_ref, gw_ref, pw_ref, eg_ref, eu_ref, ed_ref,
    rot_t_ref, rot_b_ref,
    mix_ref, moe_ref,
    w_in, w_out, w_eg, w_eu, w_ed,
    xn, xe, rq, rk, vv, gg, lo, rot_c, rot_s, c_col, c_row,
    sel0, sel1, perm,
    p1s, p1r, p2s, p2r, r1s, r1r, r2s, r2r,
    acc_g, acc_u, hid,
    st_s, st_r, tot_s, tot_r, h_in,
    sib_s, sib_r, own_p, m1_r, m2_s, m2_r,
    wsem, agss, agrs, sbss, sbrs, lsem,
    p1ss, p1rs, p2ss, p2rs, r1ss, r1rs, r2ss, r2rs,
    stss, strs, ttss, ttrs, rsss, rsrs, m1ss, m1rs, m2ss, m2rs,
):
    n_ep, zn, xnn, tok, d, ff = dims
    cw = d // CHUNKS
    slots = n_ep * 8 * CAP
    ep = lax.axis_index("ep")
    tp = lax.axis_index("tp")
    y = tp // 2
    core = tp % 2
    sib = y * 2 + (1 - core)

    def at_y(k):
        return lax.rem(y + k, 4) * 2

    right, left = at_y(1) + core, at_y(3) + core
    order = [(0, 1), (1, 0), (0, 3), (3, 0), (1, 1), (3, 3), (1, 3), (3, 1),
             (2, 0), (0, 2), (1, 2), (3, 2), (2, 1), (2, 3), (2, 2)]
    order = [(a, b) for a, b in order if a < zn and b < xnn]
    n_off = len(order)
    eps = [
        lax.rem(ep // xnn + a, zn) * xnn + lax.rem(ep % xnn + b, xnn) for a, b in order
    ]
    tps = [at_y(a) + lax.rem(core + b, 2)
           for a, b in ((1, 0), (3, 1), (1, 1), (3, 0), (2, 0), (2, 1), (0, 1))]

    loads = [
        pltpu.make_async_copy(wq_ref, w_in.at[:, pl.ds(0, KD)], wsem.at[0]),
        pltpu.make_async_copy(wk_ref, w_in.at[:, pl.ds(KD, KD)], wsem.at[1]),
        pltpu.make_async_copy(wv_ref, w_in.at[:, pl.ds(2 * KD, VD)], wsem.at[2]),
        pltpu.make_async_copy(wg_ref, w_in.at[:, pl.ds(2 * KD + VD, VD)], wsem.at[3]),
        pltpu.make_async_copy(wo_ref, w_out, wsem.at[4]),
        pltpu.make_async_copy(eg_ref, w_eg, wsem.at[5]),
        pltpu.make_async_copy(eu_ref, w_eu, wsem.at[6]),
        pltpu.make_async_copy(ed_ref, w_ed, wsem.at[7]),
    ]
    for c in loads:
        c.start()

    barrier = pltpu.get_barrier_semaphore()
    for t in eps:
        pl.semaphore_signal(barrier, inc=1, device_id={"ep": t}, device_id_type=MESH)
    for t in tps:
        pl.semaphore_signal(barrier, inc=1, device_id={"tp": t}, device_id_type=MESH)

    norm_rows(x_ref, mgain_ref, xn.at[tp], 128, 32)
    pl.semaphore_wait(barrier, n_off + 7)

    def rcopy(src, dst, ss, rs, who):
        return pltpu.make_async_remote_copy(
            src_ref=src, dst_ref=dst, send_sem=ss, recv_sem=rs,
            device_id=who, device_id_type=MESH,
        )

    def ag(direction, piece):
        half = pl.ds(64 * ((piece + direction) % 2), 64)
        if piece == 2:
            half = pl.ds(64 * direction, 64)
            block = left if direction == 0 else right
        else:
            block = tp
        ref = xn.at[block, half]
        return rcopy(ref, ref, agss.at[direction, piece], agrs.at[direction, piece],
                     {"tp": right if direction == 0 else left})

    def ag_in(direction, piece):
        half = pl.ds(64 * ((piece + direction) % 2), 64)
        if piece == 2:
            half = pl.ds(64 * direction, 64)
            block = at_y(2) + core
        else:
            block = left if direction == 0 else right
        ref = xn.at[block, half]
        return rcopy(ref, ref, agss.at[direction, piece], agrs.at[direction, piece],
                     {"tp": right if direction == 0 else left})

    def sb(k, mine=True):
        block = at_y(k) + (core if mine else 1 - core)
        ref = xn.at[block]
        return rcopy(ref, ref, sbss.at[k], sbrs.at[k], {"tp": sib})

    for piece in range(2):
        for direction in range(2):
            ag(direction, piece).start()
    sb(0).start()

    norm_rows(e_ref, egain_ref, xe, tok, min(tok, 32))
    r_io = lax.broadcasted_iota(jnp.int32, (slots, tok), 0)
    group = (r_io * 2731) >> 16
    e_of = group * 8 + (r_io & 7)
    k_of = ((r_io - group * 24) >> 3).astype(F32)
    hit0 = e_of == routes_ref[0:1, :]
    hit1 = e_of == routes_ref[1:2, :]
    hits = jnp.where(jnp.logical_or(hit0, hit1), 1.0, 0.0)
    before = lax.broadcasted_iota(jnp.int32, (tok, tok), 0) < lax.broadcasted_iota(
        jnp.int32, (tok, tok), 1
    )
    rank = dot(hits.astype(BF16), jnp.where(before, 1.0, 0.0).astype(BF16))
    here = jnp.abs(rank - k_of) < 0.5
    s0 = jnp.where(jnp.logical_and(hit0, here), 1.0, 0.0)
    s1 = jnp.where(jnp.logical_and(hit1, here), 1.0, 0.0)
    sel0[...] = s0.astype(BF16)
    sel1[...] = s1.astype(BF16)
    pick = (s0 + s1).astype(BF16)

    def ep_send(buf, into, f, ss, rs):
        for t in eps:
            rcopy(buf.at[f, t], into.at[f, ep], ss.at[f], rs.at[f], {"ep": t}).start()
        pltpu.make_async_copy(buf.at[f, ep], into.at[f, ep], lsem).start()
        pltpu.make_async_copy(buf.at[f, ep], into.at[f, ep], lsem).wait()

    def tp_send(buf, into, f, ss, rs):
        for t in tps:
            rcopy(buf.at[f, t], into.at[f, tp], ss.at[f], rs.at[f], {"tp": t}).start()
        pltpu.make_async_copy(buf.at[f, tp], into.at[f, tp], lsem).start()
        pltpu.make_async_copy(buf.at[f, tp], into.at[f, tp], lsem).wait()

    def all_of(buf, f, n, sem):
        ref = buf.at[f, pl.ds(0, n)]
        return pltpu.make_async_copy(ref, ref, sem.at[f])

    for f in range(CHUNKS):
        part = dot(pick, xe[:, f * cw:(f + 1) * cw])
        p1s[f] = part.reshape(n_ep, 24, cw).astype(BF16)
        ep_send(p1s, p1r, f, p1ss, p1rs)

    upto = lax.broadcasted_iota(jnp.int32, (128, 128), 0) <= lax.broadcasted_iota(
        jnp.int32, (128, 128), 1
    )
    inside = dot(ld_ref[...], jnp.where(upto, 1.0, 0.0), precision=HI)
    run = jnp.zeros((1, 1), F32)
    for b in range(8):
        row = inside[b:b + 1, :] + run
        c_row[b:b + 1, :] = row
        c_col[b] = jnp.transpose(jnp.broadcast_to(row, (128, 128)))
        run = run + inside[b:b + 1, 127:128]
    tot_s[...] = jnp.broadcast_to(run, (8, 128))

    def to_later(make):
        for o, t in enumerate(eps):
            @pl.when(t > ep)
            def _():
                make(o, t).start()

    def st_copy(o, t):
        return rcopy(st_s, st_r.at[ep], stss.at[o], strs.at[o], {"ep": t})

    def tt_copy(o, t):
        return rcopy(tot_s, tot_r.at[ep], ttss.at[o], ttrs.at[o], {"ep": t})

    def back(o):
        a, b = order[o]
        return lax.rem(ep // xnn + zn - a, zn) * xnn + lax.rem(ep % xnn + xnn - b, xnn)

    to_later(tt_copy)

    turn = rot_b_ref[ep]
    cb = turn[:, :KD]
    sbn = turn[:, KD:]
    for i in range(4):
        at = pl.ds(i * 256, 256)
        ct = rot_t_ref[at, :KD]
        st = rot_t_ref[at, KD:]
        rot_c[at, :] = ct * cb - st * sbn
        rot_s[at, :] = st * cb + ct * sbn

    pm_r = lax.broadcasted_iota(jnp.int32, (slots, slots), 0)
    pm_c = lax.broadcasted_iota(jnp.int32, (slots, slots), 1)
    perm[...] = jnp.where(
        pm_r == (pm_c & 7) * (n_ep * CAP) + (pm_c >> 3), 1.0, 0.0
    ).astype(BF16)

    def forward(f):
        all_of(p1r, f, n_off, p1rs).wait()
        moved = dot(perm[...], rows_of(p1r[f])).astype(BF16)
        p2s[f] = moved.reshape(8, n_ep * CAP, cw)
        tp_send(p2s, p2r, f, p2ss, p2rs)

    def project(k):
        first = pl.multiple_of(at_y(k), 2)
        rows = pl.ds(pl.multiple_of(first * 128, 256), 256)
        xb = xn[pl.ds(first, 2)].reshape(256, d)
        cos = rot_c[rows, :]
        sin = rot_s[rows, :]
        qk = dot(xb, w_in[:, :2 * KD])
        for i, ref in enumerate((rq, rk)):
            part = qk[:, i * KD:(i + 1) * KD].astype(BF16).astype(F32)
            ref[rows, :] = (part * cos + pltpu.roll(part, KD // 2, 1) * sin).astype(BF16)
        vv[rows, :] = dot(xb, w_in[:, 2 * KD:2 * KD + VD]).astype(BF16)
        gg[rows, :] = dot(xb, w_in[:, 2 * KD + VD:]).astype(BF16)

    for c in loads[:4]:
        c.wait()
    sb(0, False).wait_recv()
    project(0)
    for direction in range(2):
        ag_in(direction, 0).wait_recv()
        ag(direction, 2).start()
    forward(0)
    for direction in range(2):
        ag_in(direction, 1).wait_recv()
    sb(3).start()
    sb(1).start()
    forward(1)
    sb(3, False).wait_recv()
    project(3)
    sb(1, False).wait_recv()
    project(1)
    forward(2)
    for direction in range(2):
        ag_in(direction, 2).wait_recv()
    sb(2).start()
    forward(3)
    sb(2, False).wait_recv()
    project(2)

    state = jnp.zeros((KD, VD), F32)
    for b in range(4):
        at = pl.ds(b * 256, 256)
        left_over = jnp.exp(run - jnp.concatenate([c_col[2 * b], c_col[2 * b + 1]], axis=0))
        kw = (rk[at, :].astype(F32) * left_over).astype(BF16)
        state = state + dot_t0(kw, vv[at, :])
    st_s[...] = state.astype(BF16)

    causal = lax.broadcasted_iota(jnp.int32, (256, 256), 0) >= lax.broadcasted_iota(
        jnp.int32, (256, 256), 1
    )
    for i in range(4):
        qi = rq[pl.ds(i * 256, 256), :]
        ci = jnp.concatenate([c_col[2 * i], c_col[2 * i + 1]], axis=0)
        ci = jnp.concatenate([ci, ci], axis=1)
        out = jnp.zeros((256, VD), F32)
        for j in range(i + 1):
            at = pl.ds(j * 256, 256)
            cj = jnp.concatenate([c_row[2 * j:2 * j + 1, :], c_row[2 * j + 1:2 * j + 2, :]], axis=1)
            w = jnp.exp(jnp.minimum(ci - cj, 0.0))
            if i == j:
                w = jnp.where(causal, w, 0.0)
            dec = (dot_t1(qi, rk[at, :]) * w).astype(BF16)
            out = out + dot(dec, vv[at, :])
        lo[pl.ds(i * 256, 256), :] = out
        if i == 0:
            to_later(st_copy)

    def expert_in(f):
        all_of(p2r, f, 7, p2rs).wait()
        xf = p2r[f].reshape(slots, cw)

        @pl.loop(0, ff // 256)
        def _(n):
            at = pl.ds(pl.multiple_of(n * 256, 256), 256)
            for acc, w in ((acc_g, w_eg), (acc_u, w_eu)):
                part = dot(xf, w[f * cw:(f + 1) * cw, at])
                if f == 0:
                    acc[:, at] = part
                else:
                    acc[:, at] += part

    for c in loads[5:7]:
        c.wait()
    expert_in(0)
    expert_in(1)

    for o in range(n_off):
        src = back(o)

        @pl.when(src < ep)
        def _():
            rcopy(tot_s, tot_r.at[src], ttss.at[o], ttrs.at[o], {"ep": src}).wait_recv()
            rcopy(st_s, st_r.at[src], stss.at[o], strs.at[o], {"ep": src}).wait_recv()

    after = jnp.zeros((1, 128), F32)
    total = jnp.zeros((KD, VD), F32)
    for e in reversed(range(n_ep)):
        valid = e < ep
        coef = jnp.exp(after)
        part = st_r[e].astype(F32) * jnp.concatenate([coef, coef], axis=1)
        total = total + jnp.where(valid, part, 0.0)
        after = after + jnp.where(valid, tot_r[e, 0:1, :], 0.0)
    h_in[...] = total.astype(BF16)
    loads[4].wait()

    def partial_rows(block):
        at = pl.ds(pl.multiple_of(block * 128, 128), 128)
        col = jnp.exp(c_col[block])
        q = (rq[at, :].astype(F32) * col).astype(BF16)
        ret = lo[at, :] + dot(q, h_in[...])
        mean = jnp.mean(ret, axis=-1, keepdims=True)
        c = ret - mean
        var = jnp.mean(c * c, axis=-1, keepdims=True)
        normed = c * lax.rsqrt(var + EPSILON) * hgain_ref[...]
        g = gg[at, :].astype(F32)
        gated = (g / (1.0 + jnp.exp(-g)) * normed).astype(BF16)
        return gated

    def rs_sib(k):
        return rcopy(sib_s.at[k], sib_r.at[k], rsss.at[k], rsrs.at[k], {"tp": sib})

    def make_partial(k):
        gated = partial_rows(at_y(k) + 1 - core)
        sib_s[k] = dot(gated, w_out[...]).astype(BF16)
        gated = partial_rows(at_y(k) + core)
        rs_sib(k).start()
        own_p[k] = dot(gated, w_out[...])

    def chip_sum(k):
        rs_sib(k).wait_recv()
        return own_p[k] + sib_r[k].astype(F32)

    def m1(direction):
        src = m2_s.at[2, pl.ds(64 * direction, 64)]
        return rcopy(src, m1_r.at[direction], m1ss.at[direction], m1rs.at[direction],
                     {"tp": right if direction == 0 else left})

    def m2(direction, half):
        src = m2_s.at[direction, pl.ds(64 * half, 64)]
        return rcopy(src, m2_r.at[direction, pl.ds(64 * half, 64)],
                     m2ss.at[direction, half], m2rs.at[direction, half],
                     {"tp": right if direction == 0 else left})

    make_partial(2)
    make_partial(1)
    m2_s[2] = chip_sum(2).astype(BF16)
    make_partial(3)
    for direction in range(2):
        m1(direction).start()
    own_p[1] = chip_sum(1)
    m2_s[0, 64:128] = own_p[1, 64:128, :].astype(BF16)
    own_p[3] = chip_sum(3)
    m2_s[1, 0:64] = own_p[3, 0:64, :].astype(BF16)
    make_partial(0)
    m2(0, 1).start()
    m2(1, 0).start()

    expert_in(2)
    for direction in range(2):
        m1(direction).wait_recv()
        half = pl.ds(64 * direction, 64)
        m2_s[direction, half] = (
            own_p[1 if direction == 0 else 3, half, :] + m1_r[direction].astype(F32)
        ).astype(BF16)
    own_p[0] = chip_sum(0)
    for direction in range(2):
        m2(direction, direction).start()

    expert_in(3)

    @pl.loop(0, ff // 256)
    def _(n):
        at = pl.ds(pl.multiple_of(n * 256, 256), 256)
        g = acc_g[:, at]
        hid[:, at] = (g / (1.0 + jnp.exp(-g)) * acc_u[:, at]).astype(BF16)

    loads[7].wait()
    for f in range(CHUNKS):
        part = dot(hid[...], w_ed[:, f * cw:(f + 1) * cw]).astype(BF16)
        r1s[f] = part.reshape(8, n_ep * CAP, cw)
        tp_send(r1s, r1r, f, r1ss, r1rs)
    for f in range(CHUNKS):
        all_of(r1r, f, 7, r1rs).wait()
        moved = dot_t0(perm[...], r1r[f].reshape(slots, cw))
        r2s[f] = moved.reshape(n_ep, 24, cw).astype(BF16)
        ep_send(r2s, r2r, f, r2ss, r2rs)

    for direction in range(2):
        for half in range(2):
            m2(direction, half).wait_recv()
    mix_ref[...] = (
        own_p[0] + m2_r[0].astype(F32) + m2_r[1].astype(F32)
    ).astype(BF16)

    w0 = jnp.transpose(jnp.broadcast_to(gw_ref[...] * pw_ref[0:1, :], (128, tok)))
    w1 = jnp.transpose(jnp.broadcast_to(gw_ref[...] * pw_ref[1:2, :], (128, tok)))
    w0, w1 = w0[:, 0:1], w1[:, 0:1]
    for f in range(CHUNKS):
        all_of(r2r, f, n_off, r2rs).wait()
        got = rows_of(r2r[f])
        moe_ref[:, f * cw:(f + 1) * cw] = (
            w0 * dot_t0(sel0[...], got) + w1 * dot_t0(sel1[...], got)
        ).astype(BF16)

    for direction in range(2):
        for piece in range(3):
            ag(direction, piece).wait_send()
        m1(direction).wait_send()
        for half in range(2):
            m2(direction, half).wait_send()
    for k in range(4):
        sb(k).wait_send()
        rs_sib(k).wait_send()
    for f in range(CHUNKS):
        all_of(p1s, f, n_off, p1ss).wait()
        all_of(p2s, f, 7, p2ss).wait()
        all_of(r1s, f, 7, r1ss).wait()
        all_of(r2s, f, n_off, r2ss).wait()
    for o, t in enumerate(eps):
        @pl.when(t > ep)
        def _():
            tt_copy(o, t).wait_send()
            st_copy(o, t).wait_send()


def rotation_tables(n_ep, rows):
    half = KD // 2
    freq = (THETA ** (-np.arange(half) / half)).astype(np.float32).astype(np.float64)
    sign = np.concatenate([-np.ones(half), np.ones(half)])

    def both(positions):
        angles = np.tile(positions[:, None] * freq[None, :], (1, 2))
        return np.concatenate([np.cos(angles), np.sin(angles) * sign], axis=1)

    inner = both(np.arange(rows, dtype=np.float64))
    outer = both(rows * np.arange(n_ep, dtype=np.float64))
    return inner.astype(np.float32), outer.astype(np.float32)


def solution(mesh):
    n_ep = mesh.shape["ep"]
    zn, xnn = (4, 4) if n_ep == 16 else (n_ep, 1)

    def local(
        mixer_input, log_decay, mixer_gain, query_weight, key_weight, value_weight,
        gate_weight, head_gain, output_weight, expert_input, expert_gain, routes,
        group_weight, pair_weight, expert_gate, expert_up, expert_down,
    ):
        tok, d = expert_input.shape
        ff = expert_gate.shape[2]
        seg = log_decay.shape[0]
        slots = n_ep * 8 * CAP
        cw = d // CHUNKS
        rot_t, rot_b = rotation_tables(n_ep, seg)
        vmem = pl.BlockSpec(memory_space=pltpu.VMEM)
        hbm = pl.BlockSpec(memory_space=pl.ANY)
        in_specs = [vmem, vmem, vmem, hbm, hbm, hbm, hbm, vmem, hbm,
                    vmem, vmem, vmem, vmem, vmem, hbm, hbm, hbm, vmem, vmem]
        V = pltpu.VMEM
        DMA = pltpu.SemaphoreType.DMA
        scratch = [
            V((d, 2 * KD + 2 * VD), BF16), V((VD, d), BF16), V((d, ff), BF16),
            V((d, ff), BF16), V((ff, d), BF16),
            V((8, 128, d), BF16), V((tok, d), BF16), V((seg, KD), BF16), V((seg, KD), BF16),
            V((seg, VD), BF16), V((seg, VD), BF16), V((seg, VD), F32), V((seg, KD), F32),
            V((seg, KD), F32), V((8, 128, 128), F32), V((8, 128), F32),
            V((slots, tok), BF16), V((slots, tok), BF16), V((slots, slots), BF16),
            V((CHUNKS, n_ep, 24, cw), BF16), V((CHUNKS, n_ep, 24, cw), BF16),
            V((CHUNKS, 8, n_ep * CAP, cw), BF16), V((CHUNKS, 8, n_ep * CAP, cw), BF16),
            V((CHUNKS, 8, n_ep * CAP, cw), BF16), V((CHUNKS, 8, n_ep * CAP, cw), BF16),
            V((CHUNKS, n_ep, 24, cw), BF16), V((CHUNKS, n_ep, 24, cw), BF16),
            V((slots, ff), F32), V((slots, ff), F32), V((slots, ff), BF16),
            V((KD, VD), BF16), V((n_ep, KD, VD), BF16), V((8, 128), F32),
            V((n_ep, 8, 128), F32), V((KD, VD), BF16),
            V((4, 128, d), BF16), V((4, 128, d), BF16), V((4, 128, d), F32),
            V((2, 64, d), BF16), V((3, 128, d), BF16), V((2, 128, d), BF16),
            DMA((8,)), DMA((2, 3)), DMA((2, 3)), DMA((4,)), DMA((4,)), DMA,
            DMA((CHUNKS,)), DMA((CHUNKS,)), DMA((CHUNKS,)), DMA((CHUNKS,)),
            DMA((CHUNKS,)), DMA((CHUNKS,)), DMA((CHUNKS,)), DMA((CHUNKS,)),
            DMA((n_ep,)), DMA((n_ep,)), DMA((n_ep,)), DMA((n_ep,)),
            DMA((4,)), DMA((4,)), DMA((2,)), DMA((2,)), DMA((2, 2)), DMA((2, 2)),
        ]
        return pl.pallas_call(
            functools.partial(kernel, (n_ep, zn, xnn, tok, d, ff)),
            out_shape=(
                jax.ShapeDtypeStruct(mixer_input.shape, BF16),
                jax.ShapeDtypeStruct(expert_input.shape, BF16),
            ),
            in_specs=in_specs,
            out_specs=(vmem, vmem),
            scratch_shapes=scratch,
            compiler_params=pltpu.CompilerParams(
                collective_id=0, has_side_effects=True, vmem_limit_bytes=67043328
            ),
        )(
            mixer_input, log_decay.reshape(8, 128), mixer_gain.reshape(1, -1),
            query_weight, key_weight, value_weight, gate_weight,
            head_gain.reshape(1, -1), output_weight, expert_input,
            expert_gain.reshape(1, -1), routes.T, group_weight.reshape(1, -1),
            pair_weight.T, expert_gate[0], expert_up[0], expert_down[0],
            jnp.asarray(rot_t), jnp.asarray(rot_b[:, None, :]),
        )

    return jax.shard_map(
        local,
        mesh=mesh,
        in_specs=(
            P(("ep", "tp"), None), P("ep", "tp"), P(), P(None, "tp"), P(None, "tp"),
            P(None, "tp"), P(None, "tp"), P("tp"), P("tp", None), P(("ep", "tp"), None),
            P(), P(("ep", "tp"), None), P(("ep", "tp")), P(("ep", "tp"), None),
            P(("ep", "tp"), None, None), P(("ep", "tp"), None, None),
            P(("ep", "tp"), None, None),
        ),
        out_specs=(P(("ep", "tp"), None), P(("ep", "tp"), None)),
        check_vma=False,
    )
```

time: 236 us -> 105 us (0.44)
  Pallas kernels: 0 us -> 100 us
  waiting for transfers between devices: 78.8 us -> 0 us
  local copies, waits for them, and re-layouts: 41.7 us -> 3.76 us
  matrix products: 36.1 us -> 0 us
  starting transfers between devices: 34.6 us -> 0 us
  other arithmetic: 24.8 us -> 0 us
  between operations: 16.5 us -> 0.65 us
  loops' own time: 2.79 us -> 0 us
    pallas_call x0 -> x1, Pallas kernels: none -> 100 us  [local(): pl.pallas_call(functools.partial(kernel, (n_ep, zn, xnn, tok, d, ff)), ou...]
    all_to_all x5 -> x0, waiting for transfers between devices: 78.8 us -> none  [the longest x2 41.3 us: joined_exchange(): lax.all_to_all(blocks, axis, split_axis=0, concat_axis=0, tiled=True)]
    dot_general x13 -> x0, matrix products: 36.1 us -> none  [the longest x1 9.28 us: token_mixer(): jnp.dot(gated, output_weight, preferred_element_type=jnp.float32)]
    all_to_all x5 -> x0, starting transfers between devices: 34.6 us -> none  [the longest x2 16.8 us: joined_exchange(): lax.all_to_all(blocks, axis, split_axis=0, concat_axis=0, tiled=True)]
    another operation x13 -> x0, local copies, waits for them, and re-layouts: 12 us -> none  [the longest x1 5.16 us: joined_exchange(): blocks = blocks.reshape(-1, *inside)]
    reduce_sum x8 -> x0, other arithmetic: 11.4 us -> none  [the longest x1 3.93 us: expert_mixture(): jnp.sum(returned_rows * mixing[:, :, None], axis=1).astype(jnp.bfloat16)]
    gather x3 -> x0, local copies, waits for them, and re-layouts: 9.48 us -> none  [the longest x2 7.15 us: expert_mixture(): normed[slot_source]]
    slice x15 -> x0, local copies, waits for them, and re-layouts: 5.13 us -> none  [the longest x4 2.37 us: block_step(): span_total = cumulative[-1]]
  transfers between devices with their start and end apart: 6 -> 0, of which waited for: 4 -> 0; matrix products, arithmetic and copies ran while one was open for 29% -> 0% of each run, Pallas kernels for 0% -> 0%
where the time goes in v1:
time: 105 us; the launch traced here: 104 us
  Pallas kernels  100 us (95%)
  local copies, waits for them, and re-layouts  3.76 us (4%)
    pallas_call x1, Pallas kernels, local(): pl.pallas_call(functools.partial(kernel, (n_ep, zn, xnn, tok, d, ff)), ou...  100 us
    unnamed x2, local copies, waits for them, and re-layouts  3.76 us

profile of v1, /device:TPU:1, one launch (start us, length us, event | category | flops | bytes accessed | tf_op | source)
XLA Modules:
  0.0 104.5 jit_solution(704742267417187812)
XLA Ops:
  0.6 100.1 %shard_map.194 = (bf16[128,2048]{1,0:T(8,128)(2,1)}, bf16[128,2048]{1,0:T(8,128)(2,1)}) custom-call(bf16[128,2048]{1,0:T(8,128)(2,1)} %x_ref.1, f32[8,128]{1,0:T(8,128)} %bitcast.15, f32[1,2048]{1,0:T(1,128)} %bitcast.13, bf16[2048,128]{1,0:T(8,128)(2,1)} %wq_ref.1, bf16[2048,128]{1,0:T(8,128)(2,1)} %wk_ref.1, bf16[2048,256]{1,0:T(8,128)(2,1)} %wv_ref.1, ...), custom_call_target="tpu_custom_call" | custom-call | tf_op jit(solution)/shard_map/pallas_call | solution.py:524
  100.7 1.9 %copy.23 = bf16[128,2048]{1,0:T(8,128)(2,1)} copy(bf16[128,2048]{1,0:T(8,128)(2,1)} %get-tuple-element.4) | data formatting | bytes 1048576
  102.6 1.9 %copy.24 = bf16[128,2048]{1,0:T(8,128)(2,1)} copy(bf16[128,2048]{1,0:T(8,128)(2,1)} %get-tuple-element.5) | data formatting | bytes 1048576

commit v2 on v1

--- a/solution.py
+++ b/solution.py
@@ -54,16 +54,17 @@
     e_ref, egain_ref, routes_ref, gw_ref, pw_ref, eg_ref, eu_ref, ed_ref,
     rot_t_ref, rot_b_ref,
     mix_ref, moe_ref,
+    x_v, e_v, rot_v, mix_v, moe_v,
     w_in, w_out, w_eg, w_eu, w_ed,
     xn, xe, rq, rk, vv, gg, lo, rot_c, rot_s, c_col, c_row,
     sel0, sel1, perm,
     p1s, p1r, p2s, p2r, r1s, r1r, r2s, r2r,
     acc_g, acc_u, hid,
-    st_s, st_r, tot_s, tot_r, h_in,
+    sx_s, sx_r, sz_s, sz_r, tot_s, tot_r, h_in, h_b,
     sib_s, sib_r, own_p, m1_r, m2_s, m2_r,
     wsem, agss, agrs, sbss, sbrs, lsem,
     p1ss, p1rs, p2ss, p2rs, r1ss, r1rs, r2ss, r2rs,
-    stss, strs, ttss, ttrs, rsss, rsrs, m1ss, m1rs, m2ss, m2rs,
+    sxss, sxrs, szss, szrs, ttss, ttrs, osem, rsss, rsrs, m1ss, m1rs, m2ss, m2rs,
 ):
     n_ep, zn, xnn, tok, d, ff = dims
     cw = d // CHUNKS
@@ -98,7 +99,12 @@
         pltpu.make_async_copy(eu_ref, w_eu, wsem.at[6]),
         pltpu.make_async_copy(ed_ref, w_ed, wsem.at[7]),
     ]
-    for c in loads:
+    first = [
+        pltpu.make_async_copy(x_ref, x_v, wsem.at[8]),
+        pltpu.make_async_copy(e_ref, e_v, wsem.at[9]),
+        pltpu.make_async_copy(rot_t_ref, rot_v, wsem.at[10]),
+    ]
+    for c in first + loads:
         c.start()
 
     barrier = pltpu.get_barrier_semaphore()
@@ -107,7 +113,8 @@
     for t in tps:
         pl.semaphore_signal(barrier, inc=1, device_id={"tp": t}, device_id_type=MESH)
 
-    norm_rows(x_ref, mgain_ref, xn.at[tp], 128, 32)
+    first[0].wait()
+    norm_rows(x_v, mgain_ref, xn.at[tp], 128, 32)
     pl.semaphore_wait(barrier, n_off + 7)
 
     def rcopy(src, dst, ss, rs, who):
@@ -148,7 +155,8 @@
             ag(direction, piece).start()
     sb(0).start()
 
-    norm_rows(e_ref, egain_ref, xe, tok, min(tok, 32))
+    first[1].wait()
+    norm_rows(e_v, egain_ref, xe, tok, min(tok, 32))
     r_io = lax.broadcasted_iota(jnp.int32, (slots, tok), 0)
     group = (r_io * 2731) >> 16
     e_of = group * 8 + (r_io & 7)
@@ -163,8 +171,6 @@
     here = jnp.abs(rank - k_of) < 0.5
     s0 = jnp.where(jnp.logical_and(hit0, here), 1.0, 0.0)
     s1 = jnp.where(jnp.logical_and(hit1, here), 1.0, 0.0)
-    sel0[...] = s0.astype(BF16)
-    sel1[...] = s1.astype(BF16)
     pick = (s0 + s1).astype(BF16)
 
     def ep_send(buf, into, f, ss, rs):
@@ -200,31 +206,30 @@
         run = run + inside[b:b + 1, 127:128]
     tot_s[...] = jnp.broadcast_to(run, (8, 128))
 
-    def to_later(make):
-        for o, t in enumerate(eps):
-            @pl.when(t > ep)
-            def _():
-                make(o, t).start()
-
-    def st_copy(o, t):
-        return rcopy(st_s, st_r.at[ep], stss.at[o], strs.at[o], {"ep": t})
-
-    def tt_copy(o, t):
-        return rcopy(tot_s, tot_r.at[ep], ttss.at[o], ttrs.at[o], {"ep": t})
-
-    def back(o):
-        a, b = order[o]
-        return lax.rem(ep // xnn + zn - a, zn) * xnn + lax.rem(ep % xnn + xnn - b, xnn)
-
-    to_later(tt_copy)
-
+    def tt_copy(o):
+        return rcopy(tot_s, tot_r.at[ep], ttss.at[o], ttrs.at[o], {"ep": eps[o]})
+
+    def sx_copy(b):
+        x_me = ep % xnn
+        return rcopy(sx_s, sx_r.at[x_me], sxss.at[b], sxrs.at[b],
+                     {"ep": ep - x_me + lax.rem(x_me + b, xnn)})
+
+    def sz_copy(a):
+        return rcopy(sz_s, sz_r.at[ep // xnn], szss.at[a], szrs.at[a],
+                     {"ep": lax.rem(ep // xnn + a, zn) * xnn + ep % xnn})
+
+    for o in range(n_off):
+        tt_copy(o).start()
+    tot_r[ep] = tot_s[...]
+
+    first[2].wait()
     turn = rot_b_ref[ep]
     cb = turn[:, :KD]
     sbn = turn[:, KD:]
     for i in range(4):
         at = pl.ds(i * 256, 256)
-        ct = rot_t_ref[at, :KD]
-        st = rot_t_ref[at, KD:]
+        ct = rot_v[at, :KD]
+        st = rot_v[at, KD:]
         rot_c[at, :] = ct * cb - st * sbn
         rot_s[at, :] = st * cb + ct * sbn
 
@@ -234,11 +239,21 @@
         pm_r == (pm_c & 7) * (n_ep * CAP) + (pm_c >> 3), 1.0, 0.0
     ).astype(BF16)
 
+    sel0[...] = dot(perm[...], s0.astype(BF16)).astype(BF16)
+    sel1[...] = dot(perm[...], s1.astype(BF16)).astype(BF16)
+
+    def relay(f, got, got_sem, buf, into, ss, rs):
+        all_of(got, f, n_off, got_sem).wait()
+        moved = dot(perm[...], rows_of(got[f])).astype(BF16)
+        buf[f] = moved.reshape(8, n_ep * CAP, cw)
+        tp_send(buf, into, f, ss, rs)
+
     def forward(f):
-        all_of(p1r, f, n_off, p1rs).wait()
-        moved = dot(perm[...], rows_of(p1r[f])).astype(BF16)
-        p2s[f] = moved.reshape(8, n_ep * CAP, cw)
-        tp_send(p2s, p2r, f, p2ss, p2rs)
+        relay(f, p1r, p1rs, p2s, p2r, p2ss, p2rs)
+
+    def moe_out(f):
+        return pltpu.make_async_copy(
+            moe_v.at[f], moe_ref.at[:, pl.ds(f * cw, cw)], osem.at[f])
 
     def project(k):
         first = pl.multiple_of(at_y(k), 2)
@@ -284,11 +299,15 @@
         left_over = jnp.exp(run - jnp.concatenate([c_col[2 * b], c_col[2 * b + 1]], axis=0))
         kw = (rk[at, :].astype(F32) * left_over).astype(BF16)
         state = state + dot_t0(kw, vv[at, :])
-    st_s[...] = state.astype(BF16)
+    sx_s[...] = state.astype(BF16)
+    sx_r[ep % xnn] = state.astype(BF16)
 
     causal = lax.broadcasted_iota(jnp.int32, (256, 256), 0) >= lax.broadcasted_iota(
         jnp.int32, (256, 256), 1
     )
+    for b in range(1, xnn):
+        sx_copy(b).start()
+
     for i in range(4):
         qi = rq[pl.ds(i * 256, 256), :]
         ci = jnp.concatenate([c_col[2 * i], c_col[2 * i + 1]], axis=0)
@@ -303,12 +322,10 @@
             dec = (dot_t1(qi, rk[at, :]) * w).astype(BF16)
             out = out + dot(dec, vv[at, :])
         lo[pl.ds(i * 256, 256), :] = out
-        if i == 0:
-            to_later(st_copy)
 
     def expert_in(f):
         all_of(p2r, f, 7, p2rs).wait()
-        xf = p2r[f].reshape(slots, cw)
+        xf = dot_t0(perm[...], p2r[f].reshape(slots, cw)).astype(BF16)
 
         @pl.loop(0, ff // 256)
         def _(n):
@@ -323,39 +340,58 @@
     for c in loads[5:7]:
         c.wait()
     expert_in(0)
+
+    def lanes(v):
+        return jnp.concatenate([v, v], axis=1)
+
+    for o in range(n_off):
+        tt_copy(o).wait_recv()
+    for b in range(1, xnn):
+        sx_copy(b).wait_recv()
+    zero = jnp.zeros((1, 128), F32)
+    z_me, x_me = ep // xnn, ep % xnn
+    row = z_me * xnn
+    row_state = jnp.zeros((KD, VD), F32)
+    my_state = jnp.zeros((KD, VD), F32)
+    row_log, my_log = zero, zero
+    for i in reversed(range(xnn)):
+        t = tot_r[row + i, 0:1, :]
+        part = sx_r[i].astype(F32)
+        row_state = row_state + part * lanes(jnp.exp(row_log))
+        row_log = row_log + t
+        my_state = my_state + jnp.where(i < x_me, part * lanes(jnp.exp(my_log)), 0.0)
+        my_log = my_log + jnp.where(i < x_me, t, 0.0)
+    sz_s[...] = row_state.astype(BF16)
+    sz_r[z_me] = jnp.zeros((KD, VD), BF16)
+    h_in[...] = my_state
+    for a in range(1, zn):
+        sz_copy(a).start()
     expert_in(1)
-
-    for o in range(n_off):
-        src = back(o)
-
-        @pl.when(src < ep)
-        def _():
-            rcopy(tot_s, tot_r.at[src], ttss.at[o], ttrs.at[o], {"ep": src}).wait_recv()
-            rcopy(st_s, st_r.at[src], stss.at[o], strs.at[o], {"ep": src}).wait_recv()
-
-    after = jnp.zeros((1, 128), F32)
-    total = jnp.zeros((KD, VD), F32)
-    for e in reversed(range(n_ep)):
-        valid = e < ep
-        coef = jnp.exp(after)
-        part = st_r[e].astype(F32) * jnp.concatenate([coef, coef], axis=1)
-        total = total + jnp.where(valid, part, 0.0)
-        after = after + jnp.where(valid, tot_r[e, 0:1, :], 0.0)
-    h_in[...] = total.astype(BF16)
+    for a in range(1, zn):
+        sz_copy(a).wait_recv()
+    before_rows = jnp.zeros((KD, VD), F32)
+    z_log = zero
+    for i in reversed(range(zn)):
+        t = zero
+        for j in range(xnn):
+            t = t + tot_r[i * xnn + j, 0:1, :]
+        part = sz_r[i].astype(F32) * lanes(jnp.exp(z_log))
+        before_rows = before_rows + jnp.where(i < z_me, part, 0.0)
+        z_log = z_log + jnp.where(i < z_me, t, 0.0)
+    h_b[...] = (h_in[...] + before_rows * lanes(jnp.exp(my_log))).astype(BF16)
     loads[4].wait()
 
     def partial_rows(block):
         at = pl.ds(pl.multiple_of(block * 128, 128), 128)
         col = jnp.exp(c_col[block])
         q = (rq[at, :].astype(F32) * col).astype(BF16)
-        ret = lo[at, :] + dot(q, h_in[...])
+        ret = lo[at, :] + dot(q, h_b[...])
         mean = jnp.mean(ret, axis=-1, keepdims=True)
         c = ret - mean
         var = jnp.mean(c * c, axis=-1, keepdims=True)
         normed = c * lax.rsqrt(var + EPSILON) * hgain_ref[...]
         g = gg[at, :].astype(F32)
-        gated = (g / (1.0 + jnp.exp(-g)) * normed).astype(BF16)
-        return gated
+        return (g / (1.0 + jnp.exp(-g)) * normed).astype(BF16)
 
     def rs_sib(k):
         return rcopy(sib_s.at[k], sib_r.at[k], rsss.at[k], rsrs.at[k], {"tp": sib})
@@ -388,60 +424,60 @@
     make_partial(3)
     for direction in range(2):
         m1(direction).start()
+    expert_in(2)
     own_p[1] = chip_sum(1)
     m2_s[0, 64:128] = own_p[1, 64:128, :].astype(BF16)
     own_p[3] = chip_sum(3)
     m2_s[1, 0:64] = own_p[3, 0:64, :].astype(BF16)
-    make_partial(0)
+    expert_in(3)
     m2(0, 1).start()
     m2(1, 0).start()
 
-    expert_in(2)
+    @pl.loop(0, ff // 256)
+    def _(n):
+        at = pl.ds(pl.multiple_of(n * 256, 256), 256)
+        g = acc_g[:, at]
+        hid[:, at] = (g / (1.0 + jnp.exp(-g)) * acc_u[:, at]).astype(BF16)
+
+    loads[7].wait()
+    for f in range(CHUNKS):
+        part = dot(hid[...], w_ed[:, f * cw:(f + 1) * cw])
+        r1s[f] = part.reshape(n_ep, 24, cw).astype(BF16)
+        ep_send(r1s, r1r, f, r1ss, r1rs)
+
     for direction in range(2):
         m1(direction).wait_recv()
         half = pl.ds(64 * direction, 64)
         m2_s[direction, half] = (
             own_p[1 if direction == 0 else 3, half, :] + m1_r[direction].astype(F32)
         ).astype(BF16)
-    own_p[0] = chip_sum(0)
-    for direction in range(2):
-        m2(direction, direction).start()
-
-    expert_in(3)
-
-    @pl.loop(0, ff // 256)
-    def _(n):
-        at = pl.ds(pl.multiple_of(n * 256, 256), 256)
-        g = acc_g[:, at]
-        hid[:, at] = (g / (1.0 + jnp.exp(-g)) * acc_u[:, at]).astype(BF16)
-
-    loads[7].wait()
-    for f in range(CHUNKS):
-        part = dot(hid[...], w_ed[:, f * cw:(f + 1) * cw]).astype(BF16)
-        r1s[f] = part.reshape(8, n_ep * CAP, cw)
-        tp_send(r1s, r1r, f, r1ss, r1rs)
-    for f in range(CHUNKS):
-        all_of(r1r, f, 7, r1rs).wait()
-        moved = dot_t0(perm[...], r1r[f].reshape(slots, cw))
-        r2s[f] = moved.reshape(n_ep, 24, cw).astype(BF16)
-        ep_send(r2s, r2r, f, r2ss, r2rs)
-
-    for direction in range(2):
-        for half in range(2):
-            m2(direction, half).wait_recv()
-    mix_ref[...] = (
-        own_p[0] + m2_r[0].astype(F32) + m2_r[1].astype(F32)
-    ).astype(BF16)
-
     w0 = jnp.transpose(jnp.broadcast_to(gw_ref[...] * pw_ref[0:1, :], (128, tok)))
     w1 = jnp.transpose(jnp.broadcast_to(gw_ref[...] * pw_ref[1:2, :], (128, tok)))
     w0, w1 = w0[:, 0:1], w1[:, 0:1]
+    for direction in range(2):
+        m2(direction, direction).start()
+    make_partial(0)
+    own_p[0] = chip_sum(0)
+
     for f in range(CHUNKS):
-        all_of(r2r, f, n_off, r2rs).wait()
-        got = rows_of(r2r[f])
-        moe_ref[:, f * cw:(f + 1) * cw] = (
+        relay(f, r1r, r1rs, r2s, r2r, r2ss, r2rs)
+
+    for direction in range(2):
+        for half in range(2):
+            m2(direction, half).wait_recv()
+    mix_v[...] = (
+        own_p[0] + m2_r[0].astype(F32) + m2_r[1].astype(F32)
+    ).astype(BF16)
+    mix_out = pltpu.make_async_copy(mix_v, mix_ref, wsem.at[0])
+    mix_out.start()
+
+    for f in range(CHUNKS):
+        all_of(r2r, f, 7, r2rs).wait()
+        got = r2r[f].reshape(slots, cw)
+        moe_v[f] = (
             w0 * dot_t0(sel0[...], got) + w1 * dot_t0(sel1[...], got)
         ).astype(BF16)
+        moe_out(f).start()
 
     for direction in range(2):
         for piece in range(3):
@@ -455,13 +491,38 @@
     for f in range(CHUNKS):
         all_of(p1s, f, n_off, p1ss).wait()
         all_of(p2s, f, 7, p2ss).wait()
-        all_of(r1s, f, 7, r1ss).wait()
-        all_of(r2s, f, n_off, r2ss).wait()
-    for o, t in enumerate(eps):
-        @pl.when(t > ep)
-        def _():
-            tt_copy(o, t).wait_send()
-            st_copy(o, t).wait_send()
+        all_of(r1s, f, n_off, r1ss).wait()
+        all_of(r2s, f, 7, r2ss).wait()
+    for o in range(n_off):
+        tt_copy(o).wait_send()
+    for b in range(1, xnn):
+        sx_copy(b).wait_send()
+    for a in range(1, zn):
+        sz_copy(a).wait_send()
+    mix_out.wait()
+    for f in range(CHUNKS):
+        moe_out(f).wait()
+
+
+def place(a_ref, b_ref, a_out, b_out, buf, in_sem, out_sem):
+    parts = 2
+    rows = a_ref.shape[0] // parts
+    pairs = [(a_ref, a_out, i) for i in range(parts)] + [(b_ref, b_out, i) for i in range(parts)]
+    ins = [
+        pltpu.make_async_copy(src.at[pl.ds(i * rows, rows)], buf.at[n], in_sem.at[n])
+        for n, (src, _, i) in enumerate(pairs)
+    ]
+    outs = [
+        pltpu.make_async_copy(buf.at[n], dst.at[pl.ds(i * rows, rows)], out_sem.at[n])
+        for n, (_, dst, i) in enumerate(pairs)
+    ]
+    for c in ins:
+        c.start()
+    for c, o in zip(ins, outs):
+        c.wait()
+        o.start()
+    for o in outs:
+        o.wait()
 
 
 def rotation_tables(n_ep, rows):
@@ -495,11 +556,13 @@
         rot_t, rot_b = rotation_tables(n_ep, seg)
         vmem = pl.BlockSpec(memory_space=pltpu.VMEM)
         hbm = pl.BlockSpec(memory_space=pl.ANY)
-        in_specs = [vmem, vmem, vmem, hbm, hbm, hbm, hbm, vmem, hbm,
-                    vmem, vmem, vmem, vmem, vmem, hbm, hbm, hbm, vmem, vmem]
+        in_specs = [hbm, vmem, vmem, hbm, hbm, hbm, hbm, vmem, hbm,
+                    hbm, vmem, vmem, vmem, vmem, hbm, hbm, hbm, hbm, vmem]
         V = pltpu.VMEM
         DMA = pltpu.SemaphoreType.DMA
         scratch = [
+            V((128, d), BF16), V((tok, d), BF16), V((seg, 2 * KD), F32), V((128, d), BF16),
+            V((CHUNKS, tok, cw), BF16),
             V((d, 2 * KD + 2 * VD), BF16), V((VD, d), BF16), V((d, ff), BF16),
             V((d, ff), BF16), V((ff, d), BF16),
             V((8, 128, d), BF16), V((tok, d), BF16), V((seg, KD), BF16), V((seg, KD), BF16),
@@ -508,27 +571,28 @@
             V((slots, tok), BF16), V((slots, tok), BF16), V((slots, slots), BF16),
             V((CHUNKS, n_ep, 24, cw), BF16), V((CHUNKS, n_ep, 24, cw), BF16),
             V((CHUNKS, 8, n_ep * CAP, cw), BF16), V((CHUNKS, 8, n_ep * CAP, cw), BF16),
+            V((CHUNKS, n_ep, 24, cw), BF16), V((CHUNKS, n_ep, 24, cw), BF16),
             V((CHUNKS, 8, n_ep * CAP, cw), BF16), V((CHUNKS, 8, n_ep * CAP, cw), BF16),
-            V((CHUNKS, n_ep, 24, cw), BF16), V((CHUNKS, n_ep, 24, cw), BF16),
             V((slots, ff), F32), V((slots, ff), F32), V((slots, ff), BF16),
-            V((KD, VD), BF16), V((n_ep, KD, VD), BF16), V((8, 128), F32),
-            V((n_ep, 8, 128), F32), V((KD, VD), BF16),
+            V((KD, VD), BF16), V((xnn, KD, VD), BF16), V((KD, VD), BF16), V((zn, KD, VD), BF16),
+            V((8, 128), F32), V((n_ep, 8, 128), F32), V((KD, VD), F32), V((KD, VD), BF16),
             V((4, 128, d), BF16), V((4, 128, d), BF16), V((4, 128, d), F32),
             V((2, 64, d), BF16), V((3, 128, d), BF16), V((2, 128, d), BF16),
-            DMA((8,)), DMA((2, 3)), DMA((2, 3)), DMA((4,)), DMA((4,)), DMA,
+            DMA((11,)), DMA((2, 3)), DMA((2, 3)), DMA((4,)), DMA((4,)), DMA,
             DMA((CHUNKS,)), DMA((CHUNKS,)), DMA((CHUNKS,)), DMA((CHUNKS,)),
             DMA((CHUNKS,)), DMA((CHUNKS,)), DMA((CHUNKS,)), DMA((CHUNKS,)),
-            DMA((n_ep,)), DMA((n_ep,)), DMA((n_ep,)), DMA((n_ep,)),
+            DMA((xnn,)), DMA((xnn,)), DMA((zn,)), DMA((zn,)), DMA((n_ep,)), DMA((n_ep,)),
+            DMA((CHUNKS,)),
             DMA((4,)), DMA((4,)), DMA((2,)), DMA((2,)), DMA((2, 2)), DMA((2, 2)),
         ]
-        return pl.pallas_call(
+        mixed, moe = pl.pallas_call(
             functools.partial(kernel, (n_ep, zn, xnn, tok, d, ff)),
             out_shape=(
                 jax.ShapeDtypeStruct(mixer_input.shape, BF16),
                 jax.ShapeDtypeStruct(expert_input.shape, BF16),
             ),
             in_specs=in_specs,
-            out_specs=(vmem, vmem),
+            out_specs=(hbm, hbm),
             scratch_shapes=scratch,
             compiler_params=pltpu.CompilerParams(
                 collective_id=0, has_side_effects=True, vmem_limit_bytes=67043328
@@ -541,6 +605,17 @@
             pair_weight.T, expert_gate[0], expert_up[0], expert_down[0],
             jnp.asarray(rot_t), jnp.asarray(rot_b[:, None, :]),
         )
+        rows = mixed.shape[0] // 2
+        return pl.pallas_call(
+            place,
+            out_shape=(
+                jax.ShapeDtypeStruct(mixed.shape, BF16),
+                jax.ShapeDtypeStruct(moe.shape, BF16),
+            ),
+            in_specs=[hbm, hbm],
+            out_specs=(hbm, hbm),
+            scratch_shapes=[V((4, rows, d), BF16), DMA((4,)), DMA((4,))],
+        )(mixed, moe)
 
     return jax.shard_map(
         local,

time: 105 us -> 88.6 us (0.84)
  Pallas kernels: 100 us -> 87.6 us
  local copies, waits for them, and re-layouts: 3.76 us -> 0 us
    pallas_call x1, Pallas kernels: 100 us -> 85.6 us  [local(): pl.pallas_call(functools.partial(kernel, (n_ep, zn, xnn, tok, d, ff)), ou...]
    unnamed x2 -> x0, local copies, waits for them, and re-layouts: 3.76 us -> none
    pallas_call x0 -> x1, Pallas kernels: none -> 1.98 us  [local(): pl.pallas_call(place, out_shape=(jax.ShapeDtypeStruct(mixed.shape, BF16),...]
where the time goes in v2:
time: 88.6 us; the launch traced here: 88.4 us
  Pallas kernels  87.6 us (99%)
    pallas_call x1, Pallas kernels, local(): pl.pallas_call(functools.partial(kernel, (n_ep, zn, xnn, tok, d, ff)), ou...  85.6 us
    pallas_call x1, Pallas kernels, local(): pl.pallas_call(place, out_shape=(jax.ShapeDtypeStruct(mixed.shape, BF16),...  1.98 us

profile of v2, /device:TPU:1, one launch (start us, length us, event | category | flops | bytes accessed | tf_op | source)
XLA Modules:
  0.0 88.4 jit_solution(778260040979568339)
XLA Ops:
  0.6 85.6 %shard_map.194 = (bf16[128,2048]{1,0:T(8,128)(2,1)}, bf16[128,2048]{1,0:T(8,128)(2,1)}) custom-call(bf16[128,2048]{1,0:T(8,128)(2,1)} %x_ref.1, f32[8,128]{1,0:T(8,128)} %bitcast.15, f32[1,2048]{1,0:T(1,128)} %bitcast.13, bf16[2048,128]{1,0:T(8,128)(2,1)} %wq_ref.1, bf16[2048,128]{1,0:T(8,128)(2,1)} %wk_ref.1, bf16[2048,256]{1,0:T(8,128)(2,1)} %wv_ref.1, ...), custom_call_target="tpu_custom_call" | custom-call | tf_op jit(solution)/shard_map/pallas_call | solution.py:588
  86.2 2.0 %shard_map.195 = (bf16[128,2048]{1,0:T(8,128)(2,1)}, bf16[128,2048]{1,0:T(8,128)(2,1)}) custom-call(bf16[128,2048]{1,0:T(8,128)(2,1)} %get-tuple-element.4.a_ref, bf16[128,2048]{1,0:T(8,128)(2,1)} %get-tuple-element.5.b_ref), custom_call_target="tpu_custom_call" | custom-call | tf_op jit(solution)/shard_map/pallas_call | solution.py:609

commit v3 on v2

--- a/solution.py
+++ b/solution.py
@@ -13,7 +13,6 @@
 CAP = 3
 EPSILON = 1e-05
 THETA = 10000.0
-CHUNKS = 4
 MESH = pl.DeviceIdType.MESH
 F32 = jnp.float32
 BF16 = jnp.bfloat16
@@ -32,10 +31,10 @@
     return lax.dot_general(a, b, (((1,), (1,)), ((), ())), preferred_element_type=F32)
 
 
-def norm_rows(src, gain, dst, rows, step):
+def norm_rows(src, gain, dst, start, rows, step):
     @pl.loop(0, rows // step)
     def _(i):
-        at = pl.ds(pl.multiple_of(i * step, step), step)
+        at = pl.ds(pl.multiple_of(start + i * step, step), step)
         m = src[at, :].astype(F32)
         mean = jnp.mean(m, axis=-1, keepdims=True)
         c = m - mean
@@ -50,25 +49,24 @@
 
 def kernel(
     dims,
-    x_ref, ld_ref, mgain_ref, wq_ref, wk_ref, wv_ref, wg_ref, hgain_ref, wo_ref,
-    e_ref, egain_ref, routes_ref, gw_ref, pw_ref, eg_ref, eu_ref, ed_ref,
-    rot_t_ref, rot_b_ref,
+    x_ref, ld_in, mgain_in, wq_ref, wk_ref, wv_ref, wg_ref, hgain_in, wo_ref,
+    e_ref, egain_in, routes_in, gw_in, pw_in, eg_ref, eu_ref, ed_ref,
+    rot_t_ref, rot_b_in,
     mix_ref, moe_ref,
     x_v, e_v, rot_v, mix_v, moe_v,
+    ld_ref, mgain_ref, hgain_ref, egain_ref, routes_ref, gw_ref, pw_ref, rot_b_ref,
     w_in, w_out, w_eg, w_eu, w_ed,
     xn, xe, rq, rk, vv, gg, lo, rot_c, rot_s, c_col, c_row,
-    sel0, sel1, perm,
-    p1s, p1r, p2s, p2r, r1s, r1r, r2s, r2r,
-    acc_g, acc_u, hid,
+    sel, perm,
+    p1s, p1r, p2s, p2r, r1e, r1er, r1ts, r1tr, r2s, r2r, moe_a, hid,
     sx_s, sx_r, sz_s, sz_r, tot_s, tot_r, h_in, h_b,
     sib_s, sib_r, own_p, m1_r, m2_s, m2_r,
     wsem, agss, agrs, sbss, sbrs, lsem,
-    p1ss, p1rs, p2ss, p2rs, r1ss, r1rs, r2ss, r2rs,
-    sxss, sxrs, szss, szrs, ttss, ttrs, osem, rsss, rsrs, m1ss, m1rs, m2ss, m2rs,
+    p1ss, p1rs, p2ss, p2rs, r1ss, r1rs, r1tss, r1trs, r2ss, r2rs,
+    sxss, sxrs, szss, szrs, ttss, ttrs, rsss, rsrs, m1ss, m1rs, m2ss, m2rs,
 ):
     n_ep, zn, xnn, tok, d, ff = dims
-    cw = d // CHUNKS
-    slots = n_ep * 8 * CAP
+    slots = n_ep * 8
     ep = lax.axis_index("ep")
     tp = lax.axis_index("tp")
     y = tp // 2
@@ -89,6 +87,23 @@
     tps = [at_y(a) + lax.rem(core + b, 2)
            for a, b in ((1, 0), (3, 1), (1, 1), (3, 0), (2, 0), (2, 1), (0, 1))]
 
+    def load(n, src, dst):
+        return pltpu.make_async_copy(src, dst, wsem.at[n])
+
+    first = [
+        load(8, x_ref.at[pl.ds(0, 64)], x_v.at[pl.ds(0, 64)]),
+        load(9, mgain_in, mgain_ref),
+        load(10, x_ref.at[pl.ds(64, 64)], x_v.at[pl.ds(64, 64)]),
+        load(11, e_ref, e_v),
+        load(12, egain_in, egain_ref),
+        load(13, routes_in, routes_ref),
+        load(14, ld_in, ld_ref),
+        load(15, rot_t_ref, rot_v),
+        load(16, rot_b_in.at[ep], rot_b_ref),
+        load(17, hgain_in, hgain_ref),
+        load(18, gw_in, gw_ref),
+        load(19, pw_in, pw_ref),
+    ]
     loads = [
         pltpu.make_async_copy(wq_ref, w_in.at[:, pl.ds(0, KD)], wsem.at[0]),
         pltpu.make_async_copy(wk_ref, w_in.at[:, pl.ds(KD, KD)], wsem.at[1]),
@@ -99,22 +114,22 @@
         pltpu.make_async_copy(eu_ref, w_eu, wsem.at[6]),
         pltpu.make_async_copy(ed_ref, w_ed, wsem.at[7]),
     ]
-    first = [
-        pltpu.make_async_copy(x_ref, x_v, wsem.at[8]),
-        pltpu.make_async_copy(e_ref, e_v, wsem.at[9]),
-        pltpu.make_async_copy(rot_t_ref, rot_v, wsem.at[10]),
-    ]
-    for c in first + loads:
+    for c in first[:3]:
         c.start()
 
     barrier = pltpu.get_barrier_semaphore()
+    for t in tps:
+        pl.semaphore_signal(barrier, inc=1, device_id={"tp": t}, device_id_type=MESH)
     for t in eps:
         pl.semaphore_signal(barrier, inc=1, device_id={"ep": t}, device_id_type=MESH)
-    for t in tps:
-        pl.semaphore_signal(barrier, inc=1, device_id={"tp": t}, device_id_type=MESH)
-
-    first[0].wait()
-    norm_rows(x_v, mgain_ref, xn.at[tp], 128, 32)
+    for c in first[3:] + loads:
+        c.start()
+
+    for c in first[:2]:
+        c.wait()
+    norm_rows(x_v, mgain_ref, xn.at[tp], 0, 64, 32)
+    first[2].wait()
+    norm_rows(x_v, mgain_ref, xn.at[tp], 64, 64, 32)
     pl.semaphore_wait(barrier, n_off + 7)
 
     def rcopy(src, dst, ss, rs, who):
@@ -145,6 +160,11 @@
         return rcopy(ref, ref, agss.at[direction, piece], agrs.at[direction, piece],
                      {"tp": right if direction == 0 else left})
 
+    def sb_half(half, mine=True):
+        block = at_y(2) + (core if mine else 1 - core)
+        ref = xn.at[block, pl.ds(64 * half, 64)]
+        return rcopy(ref, ref, sbss.at[2 + 2 * half], sbrs.at[2 + 2 * half], {"tp": sib})
+
     def sb(k, mine=True):
         block = at_y(k) + (core if mine else 1 - core)
         ref = xn.at[block]
@@ -155,12 +175,10 @@
             ag(direction, piece).start()
     sb(0).start()
 
-    first[1].wait()
-    norm_rows(e_v, egain_ref, xe, tok, min(tok, 32))
-    r_io = lax.broadcasted_iota(jnp.int32, (slots, tok), 0)
-    group = (r_io * 2731) >> 16
-    e_of = group * 8 + (r_io & 7)
-    k_of = ((r_io - group * 24) >> 3).astype(F32)
+    for c in first[3:6]:
+        c.wait()
+    norm_rows(e_v, egain_ref, xe, 0, tok, min(tok, 32))
+    e_of = lax.broadcasted_iota(jnp.int32, (slots, tok), 0)
     hit0 = e_of == routes_ref[0:1, :]
     hit1 = e_of == routes_ref[1:2, :]
     hits = jnp.where(jnp.logical_or(hit0, hit1), 1.0, 0.0)
@@ -168,10 +186,6 @@
         jnp.int32, (tok, tok), 1
     )
     rank = dot(hits.astype(BF16), jnp.where(before, 1.0, 0.0).astype(BF16))
-    here = jnp.abs(rank - k_of) < 0.5
-    s0 = jnp.where(jnp.logical_and(hit0, here), 1.0, 0.0)
-    s1 = jnp.where(jnp.logical_and(hit1, here), 1.0, 0.0)
-    pick = (s0 + s1).astype(BF16)
 
     def ep_send(buf, into, f, ss, rs):
         for t in eps:
@@ -189,11 +203,18 @@
         ref = buf.at[f, pl.ds(0, n)]
         return pltpu.make_async_copy(ref, ref, sem.at[f])
 
-    for f in range(CHUNKS):
-        part = dot(pick, xe[:, f * cw:(f + 1) * cw])
-        p1s[f] = part.reshape(n_ep, 24, cw).astype(BF16)
-        ep_send(p1s, p1r, f, p1ss, p1rs)
-
+    for k in range(CAP):
+        here = jnp.abs(rank - float(k)) < 0.5
+        s0 = jnp.where(jnp.logical_and(hit0, here), 1.0, 0.0)
+        s1 = jnp.where(jnp.logical_and(hit1, here), 1.0, 0.0)
+        sel[k, 0] = s0.astype(BF16)
+        sel[k, 1] = s1.astype(BF16)
+        part = dot((s0 + s1).astype(BF16), xe[...])
+        p1s[k] = part.reshape(n_ep, 8, d).astype(BF16)
+        ep_send(p1s, p1r, k, p1ss, p1rs)
+
+    for c in first[6:]:
+        c.wait()
     upto = lax.broadcasted_iota(jnp.int32, (128, 128), 0) <= lax.broadcasted_iota(
         jnp.int32, (128, 128), 1
     )
@@ -222,8 +243,7 @@
         tt_copy(o).start()
     tot_r[ep] = tot_s[...]
 
-    first[2].wait()
-    turn = rot_b_ref[ep]
+    turn = rot_b_ref[...]
     cb = turn[:, :KD]
     sbn = turn[:, KD:]
     for i in range(4):
@@ -236,29 +256,25 @@
     pm_r = lax.broadcasted_iota(jnp.int32, (slots, slots), 0)
     pm_c = lax.broadcasted_iota(jnp.int32, (slots, slots), 1)
     perm[...] = jnp.where(
-        pm_r == (pm_c & 7) * (n_ep * CAP) + (pm_c >> 3), 1.0, 0.0
+        pm_r == (pm_c & 7) * n_ep + (pm_c >> 3), 1.0, 0.0
     ).astype(BF16)
 
-    sel0[...] = dot(perm[...], s0.astype(BF16)).astype(BF16)
-    sel1[...] = dot(perm[...], s1.astype(BF16)).astype(BF16)
+    for k in range(1, CAP):
+        for j in range(2):
+            sel[k, j] = dot(perm[...], sel[k, j]).astype(BF16)
 
     def relay(f, got, got_sem, buf, into, ss, rs):
         all_of(got, f, n_off, got_sem).wait()
         moved = dot(perm[...], rows_of(got[f])).astype(BF16)
-        buf[f] = moved.reshape(8, n_ep * CAP, cw)
+        buf[f] = moved.reshape(8, n_ep, d)
         tp_send(buf, into, f, ss, rs)
 
     def forward(f):
         relay(f, p1r, p1rs, p2s, p2r, p2ss, p2rs)
 
-    def moe_out(f):
-        return pltpu.make_async_copy(
-            moe_v.at[f], moe_ref.at[:, pl.ds(f * cw, cw)], osem.at[f])
-
-    def project(k):
-        first = pl.multiple_of(at_y(k), 2)
-        rows = pl.ds(pl.multiple_of(first * 128, 256), 256)
-        xb = xn[pl.ds(first, 2)].reshape(256, d)
+    def project(first, count):
+        rows = pl.ds(pl.multiple_of(first * 128, 128), count * 128)
+        xb = xn[pl.ds(first, count)].reshape(count * 128, d)
         cos = rot_c[rows, :]
         sin = rot_s[rows, :]
         qk = dot(xb, w_in[:, :2 * KD])
@@ -268,10 +284,20 @@
         vv[rows, :] = dot(xb, w_in[:, 2 * KD:2 * KD + VD]).astype(BF16)
         gg[rows, :] = dot(xb, w_in[:, 2 * KD + VD:]).astype(BF16)
 
+    def state_of(part):
+        total = jnp.zeros((KD, VD), F32)
+        for k in ((0,), (1, 3), (2,))[part]:
+            first = at_y(k)
+            at = pl.ds(pl.multiple_of(first * 128, 256), 256)
+            left_over = jnp.exp(run - c_col[pl.ds(first, 2)].reshape(256, 128))
+            kw = (rk[at, :].astype(F32) * left_over).astype(BF16)
+            total = total + dot_t0(kw, vv[at, :])
+        return total
+
     for c in loads[:4]:
         c.wait()
     sb(0, False).wait_recv()
-    project(0)
+    project(at_y(0), 2)
     for direction in range(2):
         ag_in(direction, 0).wait_recv()
         ag(direction, 2).start()
@@ -282,23 +308,19 @@
     sb(1).start()
     forward(1)
     sb(3, False).wait_recv()
-    project(3)
+    project(at_y(3), 2)
     sb(1, False).wait_recv()
-    project(1)
-    forward(2)
+    project(at_y(1), 2)
     for direction in range(2):
         ag_in(direction, 2).wait_recv()
-    sb(2).start()
-    forward(3)
-    sb(2, False).wait_recv()
-    project(2)
-
-    state = jnp.zeros((KD, VD), F32)
-    for b in range(4):
-        at = pl.ds(b * 256, 256)
-        left_over = jnp.exp(run - jnp.concatenate([c_col[2 * b], c_col[2 * b + 1]], axis=0))
-        kw = (rk[at, :].astype(F32) * left_over).astype(BF16)
-        state = state + dot_t0(kw, vv[at, :])
+        sb_half(direction).start()
+    state = state_of(0) + state_of(1)
+    project(at_y(2) + core, 1)
+    for direction in range(2):
+        sb_half(direction, False).wait_recv()
+    project(at_y(2) + 1 - core, 1)
+
+    state = state + state_of(2)
     sx_s[...] = state.astype(BF16)
     sx_r[ep % xnn] = state.astype(BF16)
 
@@ -307,6 +329,7 @@
     )
     for b in range(1, xnn):
         sx_copy(b).start()
+    forward(2)
 
     for i in range(4):
         qi = rq[pl.ds(i * 256, 256), :]
@@ -323,21 +346,28 @@
             out = out + dot(dec, vv[at, :])
         lo[pl.ds(i * 256, 256), :] = out
 
-    def expert_in(f):
-        all_of(p2r, f, 7, p2rs).wait()
-        xf = dot_t0(perm[...], p2r[f].reshape(slots, cw)).astype(BF16)
+    def expert_in(k):
+        all_of(p2r, k, 7, p2rs).wait()
+        xk = p2r[k].reshape(slots, d)
 
         @pl.loop(0, ff // 256)
         def _(n):
             at = pl.ds(pl.multiple_of(n * 256, 256), 256)
-            for acc, w in ((acc_g, w_eg), (acc_u, w_eu)):
-                part = dot(xf, w[f * cw:(f + 1) * cw, at])
-                if f == 0:
-                    acc[:, at] = part
-                else:
-                    acc[:, at] += part
-
-    for c in loads[5:7]:
+            g = dot(xk, w_eg[:, at])
+            u = dot(xk, w_eu[:, at])
+            hid[:, at] = (g / (1.0 + jnp.exp(-g)) * u).astype(BF16)
+
+    def expert_out(k, along_tp):
+        h = hid[...] if along_tp else dot_t0(perm[...], hid[...]).astype(BF16)
+        for n in range(4):
+            at = pl.ds(n * (d // 4), d // 4)
+            part = dot(h, w_ed[:, n * (d // 4):(n + 1) * (d // 4)])
+            if along_tp:
+                r1ts[0, :, :, at] = part.astype(BF16).reshape(8, n_ep, d // 4)
+            else:
+                r1e[k, :, :, at] = part.reshape(n_ep, 8, d // 4).astype(BF16)
+
+    for c in loads[4:]:
         c.wait()
     expert_in(0)
 
@@ -366,7 +396,11 @@
     h_in[...] = my_state
     for a in range(1, zn):
         sz_copy(a).start()
+    expert_out(0, True)
+    tp_send(r1ts, r1tr, 0, r1tss, r1trs)
     expert_in(1)
+    expert_out(1, False)
+    ep_send(r1e, r1er, 1, r1ss, r1rs)
     for a in range(1, zn):
         sz_copy(a).wait_recv()
     before_rows = jnp.zeros((KD, VD), F32)
@@ -379,7 +413,6 @@
         before_rows = before_rows + jnp.where(i < z_me, part, 0.0)
         z_log = z_log + jnp.where(i < z_me, t, 0.0)
     h_b[...] = (h_in[...] + before_rows * lanes(jnp.exp(my_log))).astype(BF16)
-    loads[4].wait()
 
     def partial_rows(block):
         at = pl.ds(pl.multiple_of(block * 128, 128), 128)
@@ -393,12 +426,20 @@
         g = gg[at, :].astype(F32)
         return (g / (1.0 + jnp.exp(-g)) * normed).astype(BF16)
 
+    def relay_ep():
+        all_of(r1tr, 0, 7, r1trs).wait()
+        moved = dot_t0(perm[...], r1tr[0].reshape(slots, d))
+        r1e[0] = moved.reshape(n_ep, 8, d).astype(BF16)
+        ep_send(r1e, r1er, 0, r1ss, r1rs)
+
     def rs_sib(k):
         return rcopy(sib_s.at[k], sib_r.at[k], rsss.at[k], rsrs.at[k], {"tp": sib})
 
-    def make_partial(k):
+    def sib_part(k):
         gated = partial_rows(at_y(k) + 1 - core)
         sib_s[k] = dot(gated, w_out[...]).astype(BF16)
+
+    def own_part(k):
         gated = partial_rows(at_y(k) + core)
         rs_sib(k).start()
         own_p[k] = dot(gated, w_out[...])
@@ -418,32 +459,28 @@
                      m2ss.at[direction, half], m2rs.at[direction, half],
                      {"tp": right if direction == 0 else left})
 
-    make_partial(2)
-    make_partial(1)
+    sib_part(2)
+    own_part(2)
+    sib_part(1)
     m2_s[2] = chip_sum(2).astype(BF16)
-    make_partial(3)
+    own_part(1)
     for direction in range(2):
         m1(direction).start()
     expert_in(2)
+    expert_out(2, False)
     own_p[1] = chip_sum(1)
     m2_s[0, 64:128] = own_p[1, 64:128, :].astype(BF16)
+    ep_send(r1e, r1er, 2, r1ss, r1rs)
+    sib_part(3)
+    own_part(3)
+    m2(0, 1).start()
+    relay_ep()
     own_p[3] = chip_sum(3)
     m2_s[1, 0:64] = own_p[3, 0:64, :].astype(BF16)
-    expert_in(3)
-    m2(0, 1).start()
+    relay(1, r1er, r1rs, r2s, r2r, r2ss, r2rs)
     m2(1, 0).start()
-
-    @pl.loop(0, ff // 256)
-    def _(n):
-        at = pl.ds(pl.multiple_of(n * 256, 256), 256)
-        g = acc_g[:, at]
-        hid[:, at] = (g / (1.0 + jnp.exp(-g)) * acc_u[:, at]).astype(BF16)
-
-    loads[7].wait()
-    for f in range(CHUNKS):
-        part = dot(hid[...], w_ed[:, f * cw:(f + 1) * cw])
-        r1s[f] = part.reshape(n_ep, 24, cw).astype(BF16)
-        ep_send(r1s, r1r, f, r1ss, r1rs)
+    sib_part(0)
+    own_part(0)
 
     for direction in range(2):
         m1(direction).wait_recv()
@@ -456,28 +493,36 @@
     w0, w1 = w0[:, 0:1], w1[:, 0:1]
     for direction in range(2):
         m2(direction, direction).start()
-    make_partial(0)
-    own_p[0] = chip_sum(0)
-
-    for f in range(CHUNKS):
-        relay(f, r1r, r1rs, r2s, r2r, r2ss, r2rs)
-
+    relay(2, r1er, r1rs, r2s, r2r, r2ss, r2rs)
+
+    def combine(k, got):
+        for n in range(4):
+            at = pl.ds(n * (d // 4), d // 4)
+            part = w0 * dot_t0(sel[k, 0], got[:, n * (d // 4):(n + 1) * (d // 4)])
+            part = part + w1 * dot_t0(sel[k, 1], got[:, n * (d // 4):(n + 1) * (d // 4)])
+            if k == 0:
+                moe_a[:, at] = part
+            elif k == 1:
+                moe_a[:, at] += part
+            else:
+                moe_v[:, at] = (moe_a[:, at] + part).astype(BF16)
+
+    all_of(r1er, 0, n_off, r1rs).wait()
+    combine(0, rows_of(r1er[0]))
     for direction in range(2):
         for half in range(2):
             m2(direction, half).wait_recv()
     mix_v[...] = (
-        own_p[0] + m2_r[0].astype(F32) + m2_r[1].astype(F32)
+        chip_sum(0) + m2_r[0].astype(F32) + m2_r[1].astype(F32)
     ).astype(BF16)
     mix_out = pltpu.make_async_copy(mix_v, mix_ref, wsem.at[0])
     mix_out.start()
 
-    for f in range(CHUNKS):
-        all_of(r2r, f, 7, r2rs).wait()
-        got = r2r[f].reshape(slots, cw)
-        moe_v[f] = (
-            w0 * dot_t0(sel0[...], got) + w1 * dot_t0(sel1[...], got)
-        ).astype(BF16)
-        moe_out(f).start()
+    for k in range(1, CAP):
+        all_of(r2r, k, 7, r2rs).wait()
+        combine(k, r2r[k].reshape(slots, d))
+    moe_out = pltpu.make_async_copy(moe_v, moe_ref, wsem.at[1])
+    moe_out.start()
 
     for direction in range(2):
         for piece in range(3):
@@ -486,13 +531,18 @@
         for half in range(2):
             m2(direction, half).wait_send()
     for k in range(4):
+        rs_sib(k).wait_send()
+    for k in (0, 1, 3):
         sb(k).wait_send()
-        rs_sib(k).wait_send()
-    for f in range(CHUNKS):
-        all_of(p1s, f, n_off, p1ss).wait()
-        all_of(p2s, f, 7, p2ss).wait()
-        all_of(r1s, f, n_off, r1ss).wait()
-        all_of(r2s, f, 7, r2ss).wait()
+    for half in range(2):
+        sb_half(half).wait_send()
+    for k in range(CAP):
+        all_of(p1s, k, n_off, p1ss).wait()
+        all_of(p2s, k, 7, p2ss).wait()
+        all_of(r1e, k, n_off, r1ss).wait()
+        if k:
+            all_of(r2s, k, 7, r2ss).wait()
+    all_of(r1ts, 0, 7, r1tss).wait()
     for o in range(n_off):
         tt_copy(o).wait_send()
     for b in range(1, xnn):
@@ -500,8 +550,7 @@
     for a in range(1, zn):
         sz_copy(a).wait_send()
     mix_out.wait()
-    for f in range(CHUNKS):
-        moe_out(f).wait()
+    moe_out.wait()
 
 
 def place(a_ref, b_ref, a_out, b_out, buf, in_sem, out_sem):
@@ -551,38 +600,37 @@
         tok, d = expert_input.shape
         ff = expert_gate.shape[2]
         seg = log_decay.shape[0]
-        slots = n_ep * 8 * CAP
-        cw = d // CHUNKS
+        slots = n_ep * 8
         rot_t, rot_b = rotation_tables(n_ep, seg)
-        vmem = pl.BlockSpec(memory_space=pltpu.VMEM)
         hbm = pl.BlockSpec(memory_space=pl.ANY)
-        in_specs = [hbm, vmem, vmem, hbm, hbm, hbm, hbm, vmem, hbm,
-                    hbm, vmem, vmem, vmem, vmem, hbm, hbm, hbm, hbm, vmem]
+        in_specs = [hbm] * 19
         V = pltpu.VMEM
         DMA = pltpu.SemaphoreType.DMA
         scratch = [
             V((128, d), BF16), V((tok, d), BF16), V((seg, 2 * KD), F32), V((128, d), BF16),
-            V((CHUNKS, tok, cw), BF16),
+            V((tok, d), BF16),
+            V((8, 128), F32), V((1, d), F32), V((1, VD), F32), V((1, d), F32),
+            V((2, tok), jnp.int32), V((1, tok), F32), V((2, tok), F32), V((1, 2 * KD), F32),
             V((d, 2 * KD + 2 * VD), BF16), V((VD, d), BF16), V((d, ff), BF16),
             V((d, ff), BF16), V((ff, d), BF16),
             V((8, 128, d), BF16), V((tok, d), BF16), V((seg, KD), BF16), V((seg, KD), BF16),
             V((seg, VD), BF16), V((seg, VD), BF16), V((seg, VD), F32), V((seg, KD), F32),
             V((seg, KD), F32), V((8, 128, 128), F32), V((8, 128), F32),
-            V((slots, tok), BF16), V((slots, tok), BF16), V((slots, slots), BF16),
-            V((CHUNKS, n_ep, 24, cw), BF16), V((CHUNKS, n_ep, 24, cw), BF16),
-            V((CHUNKS, 8, n_ep * CAP, cw), BF16), V((CHUNKS, 8, n_ep * CAP, cw), BF16),
-            V((CHUNKS, n_ep, 24, cw), BF16), V((CHUNKS, n_ep, 24, cw), BF16),
-            V((CHUNKS, 8, n_ep * CAP, cw), BF16), V((CHUNKS, 8, n_ep * CAP, cw), BF16),
-            V((slots, ff), F32), V((slots, ff), F32), V((slots, ff), BF16),
+            V((CAP, 2, slots, tok), BF16), V((slots, slots), BF16),
+            V((CAP, n_ep, 8, d), BF16), V((CAP, n_ep, 8, d), BF16),
+            V((CAP, 8, n_ep, d), BF16), V((CAP, 8, n_ep, d), BF16),
+            V((CAP, n_ep, 8, d), BF16), V((CAP, n_ep, 8, d), BF16),
+            V((1, 8, n_ep, d), BF16), V((1, 8, n_ep, d), BF16),
+            V((CAP, 8, n_ep, d), BF16), V((CAP, 8, n_ep, d), BF16),
+            V((tok, d), F32), V((slots, ff), BF16),
             V((KD, VD), BF16), V((xnn, KD, VD), BF16), V((KD, VD), BF16), V((zn, KD, VD), BF16),
             V((8, 128), F32), V((n_ep, 8, 128), F32), V((KD, VD), F32), V((KD, VD), BF16),
             V((4, 128, d), BF16), V((4, 128, d), BF16), V((4, 128, d), F32),
             V((2, 64, d), BF16), V((3, 128, d), BF16), V((2, 128, d), BF16),
-            DMA((11,)), DMA((2, 3)), DMA((2, 3)), DMA((4,)), DMA((4,)), DMA,
-            DMA((CHUNKS,)), DMA((CHUNKS,)), DMA((CHUNKS,)), DMA((CHUNKS,)),
-            DMA((CHUNKS,)), DMA((CHUNKS,)), DMA((CHUNKS,)), DMA((CHUNKS,)),
+            DMA((20,)), DMA((2, 3)), DMA((2, 3)), DMA((5,)), DMA((5,)), DMA,
+            DMA((CAP,)), DMA((CAP,)), DMA((CAP,)), DMA((CAP,)), DMA((CAP,)), DMA((CAP,)),
+            DMA((1,)), DMA((1,)), DMA((CAP,)), DMA((CAP,)),
             DMA((xnn,)), DMA((xnn,)), DMA((zn,)), DMA((zn,)), DMA((n_ep,)), DMA((n_ep,)),
-            DMA((CHUNKS,)),
             DMA((4,)), DMA((4,)), DMA((2,)), DMA((2,)), DMA((2, 2)), DMA((2, 2)),
         ]
         mixed, moe = pl.pallas_call(

time: 88.6 us -> 84 us (0.948)
  Pallas kernels: 87.6 us -> 83.1 us
    pallas_call x1, Pallas kernels: 85.6 us -> 81.1 us  [local(): pl.pallas_call(functools.partial(kernel, (n_ep, zn, xnn, tok, d, ff)), ou...]
where the time goes in v3:
time: 84 us; the launch traced here: 83.9 us
  Pallas kernels  83.1 us (99%)
    pallas_call x1, Pallas kernels, local(): pl.pallas_call(functools.partial(kernel, (n_ep, zn, xnn, tok, d, ff)), ou...  81.1 us
    pallas_call x1, Pallas kernels, local(): pl.pallas_call(place, out_shape=(jax.ShapeDtypeStruct(mixed.shape, BF16),...  1.98 us

profile of v3, /device:TPU:1, one launch (start us, length us, event | category | flops | bytes accessed | tf_op | source)
XLA Modules:
  0.0 83.9 jit_solution(13505361832625716360)
XLA Ops:
  0.6 81.1 %shard_map.194 = (bf16[128,2048]{1,0:T(8,128)(2,1)}, bf16[128,2048]{1,0:T(8,128)(2,1)}) custom-call(bf16[128,2048]{1,0:T(8,128)(2,1)} %x_ref.1, f32[8,128]{1,0:T(8,128)} %bitcast.15, f32[1,2048]{1,0:T(1,128)} %bitcast.13, bf16[2048,128]{1,0:T(8,128)(2,1)} %wq_ref.1, bf16[2048,128]{1,0:T(8,128)(2,1)} %wk_ref.1, bf16[2048,256]{1,0:T(8,128)(2,1)} %wv_ref.1, ...), custom_call_target="tpu_custom_call" | custom-call | tf_op jit(solution)/shard_map/pallas_call | solution.py:636
  81.8 2.0 %shard_map.195 = (bf16[128,2048]{1,0:T(8,128)(2,1)}, bf16[128,2048]{1,0:T(8,128)(2,1)}) custom-call(bf16[128,2048]{1,0:T(8,128)(2,1)} %get-tuple-element.4.a_ref, bf16[128,2048]{1,0:T(8,128)(2,1)} %get-tuple-element.5.b_ref), custom_call_target="tpu_custom_call" | custom-call | tf_op jit(solution)/shard_map/pallas_call | solution.py:657

commit v4 on v3

--- a/solution.py
+++ b/solution.py
@@ -53,7 +53,7 @@
     e_ref, egain_in, routes_in, gw_in, pw_in, eg_ref, eu_ref, ed_ref,
     rot_t_ref, rot_b_in,
     mix_ref, moe_ref,
-    x_v, e_v, rot_v, mix_v, moe_v,
+    x_v, e_v, rot_v,
     ld_ref, mgain_ref, hgain_ref, egain_ref, routes_ref, gw_ref, pw_ref, rot_b_ref,
     w_in, w_out, w_eg, w_eu, w_ed,
     xn, xe, rq, rk, vv, gg, lo, rot_c, rot_s, c_col, c_row,
@@ -505,24 +505,20 @@
             elif k == 1:
                 moe_a[:, at] += part
             else:
-                moe_v[:, at] = (moe_a[:, at] + part).astype(BF16)
+                moe_ref[:, at] = (moe_a[:, at] + part).astype(BF16)
 
     all_of(r1er, 0, n_off, r1rs).wait()
     combine(0, rows_of(r1er[0]))
     for direction in range(2):
         for half in range(2):
             m2(direction, half).wait_recv()
-    mix_v[...] = (
+    mix_ref[...] = (
         chip_sum(0) + m2_r[0].astype(F32) + m2_r[1].astype(F32)
     ).astype(BF16)
-    mix_out = pltpu.make_async_copy(mix_v, mix_ref, wsem.at[0])
-    mix_out.start()
 
     for k in range(1, CAP):
         all_of(r2r, k, 7, r2rs).wait()
         combine(k, r2r[k].reshape(slots, d))
-    moe_out = pltpu.make_async_copy(moe_v, moe_ref, wsem.at[1])
-    moe_out.start()
 
     for direction in range(2):
         for piece in range(3):
@@ -549,29 +545,17 @@
         sx_copy(b).wait_send()
     for a in range(1, zn):
         sz_copy(a).wait_send()
-    mix_out.wait()
-    moe_out.wait()
-
-
-def place(a_ref, b_ref, a_out, b_out, buf, in_sem, out_sem):
-    parts = 2
-    rows = a_ref.shape[0] // parts
-    pairs = [(a_ref, a_out, i) for i in range(parts)] + [(b_ref, b_out, i) for i in range(parts)]
-    ins = [
-        pltpu.make_async_copy(src.at[pl.ds(i * rows, rows)], buf.at[n], in_sem.at[n])
-        for n, (src, _, i) in enumerate(pairs)
+
+
+def place(a_ref, b_ref, a_out, b_out, sem):
+    outs = [
+        pltpu.make_async_copy(a_ref, a_out, sem.at[0]),
+        pltpu.make_async_copy(b_ref, b_out, sem.at[1]),
     ]
-    outs = [
-        pltpu.make_async_copy(buf.at[n], dst.at[pl.ds(i * rows, rows)], out_sem.at[n])
-        for n, (_, dst, i) in enumerate(pairs)
-    ]
-    for c in ins:
+    for c in outs:
         c.start()
-    for c, o in zip(ins, outs):
+    for c in outs:
         c.wait()
-        o.start()
-    for o in outs:
-        o.wait()
 
 
 def rotation_tables(n_ep, rows):
@@ -603,12 +587,12 @@
         slots = n_ep * 8
         rot_t, rot_b = rotation_tables(n_ep, seg)
         hbm = pl.BlockSpec(memory_space=pl.ANY)
+        near = pl.BlockSpec(memory_space=pltpu.VMEM)
         in_specs = [hbm] * 19
         V = pltpu.VMEM
         DMA = pltpu.SemaphoreType.DMA
         scratch = [
-            V((128, d), BF16), V((tok, d), BF16), V((seg, 2 * KD), F32), V((128, d), BF16),
-            V((tok, d), BF16),
+            V((128, d), BF16), V((tok, d), BF16), V((seg, 2 * KD), F32),
             V((8, 128), F32), V((1, d), F32), V((1, VD), F32), V((1, d), F32),
             V((2, tok), jnp.int32), V((1, tok), F32), V((2, tok), F32), V((1, 2 * KD), F32),
             V((d, 2 * KD + 2 * VD), BF16), V((VD, d), BF16), V((d, ff), BF16),
@@ -635,15 +619,12 @@
         ]
         mixed, moe = pl.pallas_call(
             functools.partial(kernel, (n_ep, zn, xnn, tok, d, ff)),
-            out_shape=(
-                jax.ShapeDtypeStruct(mixer_input.shape, BF16),
-                jax.ShapeDtypeStruct(expert_input.shape, BF16),
-            ),
+            out_shape=(V(mixer_input.shape, BF16), V(expert_input.shape, BF16)),
             in_specs=in_specs,
-            out_specs=(hbm, hbm),
+            out_specs=(near, near),
             scratch_shapes=scratch,
             compiler_params=pltpu.CompilerParams(
-                collective_id=0, has_side_effects=True, vmem_limit_bytes=67043328
+                collective_id=0, has_side_effects=True, vmem_limit_bytes=58 * 2**20
             ),
         )(
             mixer_input, log_decay.reshape(8, 128), mixer_gain.reshape(1, -1),
@@ -653,17 +634,16 @@
             pair_weight.T, expert_gate[0], expert_up[0], expert_down[0],
             jnp.asarray(rot_t), jnp.asarray(rot_b[:, None, :]),
         )
-        rows = mixed.shape[0] // 2
         return pl.pallas_call(
             place,
             out_shape=(
                 jax.ShapeDtypeStruct(mixed.shape, BF16),
                 jax.ShapeDtypeStruct(moe.shape, BF16),
             ),
-            in_specs=[hbm, hbm],
+            in_specs=[near, near],
             out_specs=(hbm, hbm),
-            scratch_shapes=[V((4, rows, d), BF16), DMA((4,)), DMA((4,))],
-        )(mixed, moe)
+            scratch_shapes=[DMA((2,))],
+        )(*(pltpu.with_memory_space_constraint(v, pltpu.VMEM) for v in (mixed, moe)))
 
     return jax.shard_map(
         local,

time: 84 us -> 82.3 us (0.980)
  Pallas kernels: 83.1 us -> 81.4 us
    pallas_call x1, Pallas kernels: 1.98 us -> 0.99 us  [local(): pl.pallas_call(place, out_shape=(jax.ShapeDtypeStruct(mixed.shape, BF16),...]
where the time goes in v4:
time: 82.3 us; the launch traced here: 82.2 us
  Pallas kernels  81.4 us (99%)
    pallas_call x1, Pallas kernels, local(): pl.pallas_call(functools.partial(kernel, (n_ep, zn, xnn, tok, d, ff)), ou...  80.4 us

profile of v4, /device:TPU:1, one launch (start us, length us, event | category | flops | bytes accessed | tf_op | source)
XLA Modules:
  0.0 82.2 jit_solution(10142025822017298013)
XLA Ops:
  0.6 80.4 %shard_map.194 = (bf16[128,2048]{1,0:T(8,128)(2,1)S(1)}, bf16[128,2048]{1,0:T(8,128)(2,1)S(1)}) custom-call(bf16[128,2048]{1,0:T(8,128)(2,1)} %x_ref.1, f32[8,128]{1,0:T(8,128)} %bitcast.15, f32[1,2048]{1,0:T(1,128)} %bitcast.13, bf16[2048,128]{1,0:T(8,128)(2,1)} %wq_ref.1, bf16[2048,128]{1,0:T(8,128)(2,1)} %wk_ref.1, bf16[2048,256]{1,0:T(8,128)(2,1)} %wv_ref.1, ...), custom_call_target="tpu_custom_call" | custom-call | tf_op jit(solution)/shard_map/pallas_call | solution.py:620
  81.0 1.0 %shard_map.195 = (bf16[128,2048]{1,0:T(8,128)(2,1)}, bf16[128,2048]{1,0:T(8,128)(2,1)}) custom-call(bf16[128,2048]{1,0:T(8,128)(2,1)S(1)} %get-tuple-element.4.a_ref, bf16[128,2048]{1,0:T(8,128)(2,1)S(1)} %get-tuple-element.5.b_ref), custom_call_target="tpu_custom_call" | custom-call | tf_op jit(solution)/shard_map/pallas_call | solution.py:637

commit v5 on v4

--- a/solution.py
+++ b/solution.py
@@ -127,9 +127,9 @@
 
     for c in first[:2]:
         c.wait()
-    norm_rows(x_v, mgain_ref, xn.at[tp], 0, 64, 32)
+    norm_rows(x_v, mgain_ref, xn.at[tp], 0, 64, 64)
     first[2].wait()
-    norm_rows(x_v, mgain_ref, xn.at[tp], 64, 64, 32)
+    norm_rows(x_v, mgain_ref, xn.at[tp], 64, 64, 64)
     pl.semaphore_wait(barrier, n_off + 7)
 
     def rcopy(src, dst, ss, rs, who):
@@ -177,7 +177,7 @@
 
     for c in first[3:6]:
         c.wait()
-    norm_rows(e_v, egain_ref, xe, 0, tok, min(tok, 32))
+    norm_rows(e_v, egain_ref, xe, 0, tok, min(tok, 64))
     e_of = lax.broadcasted_iota(jnp.int32, (slots, tok), 0)
     hit0 = e_of == routes_ref[0:1, :]
     hit1 = e_of == routes_ref[1:2, :]
@@ -509,16 +509,17 @@
 
     all_of(r1er, 0, n_off, r1rs).wait()
     combine(0, rows_of(r1er[0]))
+
+    all_of(r2r, 1, 7, r2rs).wait()
+    combine(1, r2r[1].reshape(slots, d))
     for direction in range(2):
         for half in range(2):
             m2(direction, half).wait_recv()
     mix_ref[...] = (
         chip_sum(0) + m2_r[0].astype(F32) + m2_r[1].astype(F32)
     ).astype(BF16)
-
-    for k in range(1, CAP):
-        all_of(r2r, k, 7, r2rs).wait()
-        combine(k, r2r[k].reshape(slots, d))
+    all_of(r2r, 2, 7, r2rs).wait()
+    combine(2, r2r[2].reshape(slots, d))
 
     for direction in range(2):
         for piece in range(3):

time: 82.3 us -> 82.3 us (level)
  no operation moved by 1% of the time
where the time goes in v5:
time: 82.3 us; the launch traced here: 82.2 us
  Pallas kernels  81.4 us (99%)
    pallas_call x1, Pallas kernels, local(): pl.pallas_call(functools.partial(kernel, (n_ep, zn, xnn, tok, d, ff)), ou...  80.4 us

profile of v5, /device:TPU:1, one launch (start us, length us, event | category | flops | bytes accessed | tf_op | source)
XLA Modules:
  0.0 82.2 jit_solution(8693667330606773686)
XLA Ops:
  0.6 80.4 %shard_map.194 = (bf16[128,2048]{1,0:T(8,128)(2,1)S(1)}, bf16[128,2048]{1,0:T(8,128)(2,1)S(1)}) custom-call(bf16[128,2048]{1,0:T(8,128)(2,1)} %x_ref.1, f32[8,128]{1,0:T(8,128)} %bitcast.15, f32[1,2048]{1,0:T(1,128)} %bitcast.13, bf16[2048,128]{1,0:T(8,128)(2,1)} %wq_ref.1, bf16[2048,128]{1,0:T(8,128)(2,1)} %wk_ref.1, bf16[2048,256]{1,0:T(8,128)(2,1)} %wv_ref.1, ...), custom_call_target="tpu_custom_call" | custom-call | tf_op jit(solution)/shard_map/pallas_call | solution.py:621
  81.0 1.0 %shard_map.195 = (bf16[128,2048]{1,0:T(8,128)(2,1)}, bf16[128,2048]{1,0:T(8,128)(2,1)}) custom-call(bf16[128,2048]{1,0:T(8,128)(2,1)S(1)} %get-tuple-element.4.a_ref, bf16[128,2048]{1,0:T(8,128)(2,1)S(1)} %get-tuple-element.5.b_ref), custom_call_target="tpu_custom_call" | custom-call | tf_op jit(solution)/shard_map/pallas_call | solution.py:638
